TPU v7x, 1024 devices: a whole 4x4x32 slice. The times are simulated.
1024 devices in a mesh: row: 64 (over z, core), col: 16 (over y, x).
Axes of the slice: x: 4, y: 4, z: 32, core: 2. Of those that a mesh axis runs over, the one named last changes fastest.
Arguments:
- streams: bfloat16 [3, 1, 131072, 512], P(None, None, ('row', 'col')), may hold values from -6 to 6
- filter_taps: float32 [2, 131072, 512], P(None, ('row', 'col')), may hold values from -4 to 4
- short_taps: float32 [3, 3, 512], replicated, may hold values from -3 to 3
- skip_gain: float32 [512], replicated, may hold values from -3 to 3
- out_weight: bfloat16 [512, 4096], replicated, may hold values from -0.25 to 0.25
Outputs:
- projected: bfloat16 [1, 131072, 4096], P(None, ('row', 'col'))
All inputs are finite; a program needn't handle non-finite values.
Results may differ from a plain program's by a relative error of at most 0.0049.
Values may be sent and summed in bfloat16 or wider, within the bound.
A program may use at most 32 MiB of HBM per device.

v0:
```python
import math

import jax
import jax.numpy as jnp
from jax import lax
from jax.sharding import PartitionSpec as P

HIGHEST_PRECISION = lax.Precision.HIGHEST
EPSILON = 1e-06


def padded_2(array, sides, width):
    edges = {}
    for axis, dim in sides:
        size, length = (lax.axis_size(axis), array.shape[dim])
        up = [(i, (i + 1) % size) for i in range(size - 1)]
        last = lax.slice_in_dim(array, length - width, length, axis=dim)
        leading = lax.slice_in_dim(array, 0, width, axis=dim)
        edges[dim] = (
            lax.ppermute(last, axis, up),
            lax.ppermute(leading, axis, [(b, a) for a, b in up]),
        )
    done = []
    for _, dim in sides:
        low, high = edges[dim]
        around = [(width, width) if d in done else (0, 0) for d in range(array.ndim)]
        array = jnp.concatenate([jnp.pad(low, around), array, jnp.pad(high, around)], axis=dim)
        done.append(dim)
    return array


def in_one_piece(arrays, axis, split_dim, concat_dim, along):
    ends, at = ([], 0)
    for a in arrays[:-1]:
        at += a.shape[along]
        ends.append(at)
    both = jnp.concatenate(arrays, axis=along)
    return tuple(
        jnp.split(
            lax.all_to_all(both, axis, split_axis=split_dim, concat_axis=concat_dim, tiled=True),
            ends,
            axis=along,
        )
    )


def unit_circle(numerator, period):
    angles = 2.0 * math.pi / period * (numerator % period).astype(jnp.float32)
    return (jnp.cos(angles), jnp.sin(angles))


def complex_times(left_real, left_imag, right_real, right_imag):
    return (
        left_real * right_real - left_imag * right_imag,
        left_real * right_imag + left_imag * right_real,
    )


def complex_einsum(formula, matrix_real, matrix_imag, operand_real, operand_imag):

    def single(matrix, operand):
        return jnp.einsum(formula, matrix, operand, precision=HIGHEST_PRECISION)

    return (
        single(matrix_real, operand_real) - single(matrix_imag, operand_imag),
        single(matrix_real, operand_imag) + single(matrix_imag, operand_real),
    )


def sequence_offsets(column_count, positions):
    blocks = jnp.arange(column_count, dtype=jnp.int32)
    within = jnp.arange(positions, dtype=jnp.int32)
    return (blocks, within, positions * blocks[:, None] + within[None, :])


def forward_rows(real_part, imag_part, frequencies, length):
    column_count, positions = (real_part.shape[1], real_part.shape[4])
    blocks, within, offsets = sequence_offsets(column_count, positions)
    cos_table, sin_table = unit_circle(frequencies[:, None, None] * offsets[None], length)
    real_part, imag_part = complex_times(
        real_part, imag_part, cos_table[:, :, None, None, :], -sin_table[:, :, None, None, :]
    )
    cos_table, sin_table = unit_circle(blocks[:, None] * blocks[None, :], column_count)
    real_part, imag_part = complex_einsum(
        "mc,rcbhj->rmbhj", cos_table, -sin_table, real_part, imag_part
    )
    cos_table, sin_table = unit_circle(blocks[:, None] * within[None, :], column_count * positions)
    real_part, imag_part = complex_times(
        real_part, imag_part, cos_table[None, :, None, None, :], -sin_table[None, :, None, None, :]
    )
    cos_table, sin_table = unit_circle(within[:, None] * within[None, :], positions)
    return complex_einsum("nj,rmbhj->rmbhn", cos_table, -sin_table, real_part, imag_part)


def inverse_rows(real_part, imag_part, frequencies, length):
    column_count, positions = (real_part.shape[1], real_part.shape[4])
    blocks, within, offsets = sequence_offsets(column_count, positions)
    cos_table, sin_table = unit_circle(within[:, None] * within[None, :], positions)
    real_part, imag_part = complex_einsum(
        "jn,rmbhn->rmbhj", cos_table, sin_table, real_part, imag_part
    )
    cos_table, sin_table = unit_circle(blocks[:, None] * within[None, :], column_count * positions)
    real_part, imag_part = complex_times(
        real_part, imag_part, cos_table[None, :, None, None, :], sin_table[None, :, None, None, :]
    )
    cos_table, sin_table = unit_circle(blocks[:, None] * blocks[None, :], column_count)
    real_part, imag_part = complex_einsum(
        "cm,rmbhj->rcbhj", cos_table, sin_table, real_part, imag_part
    )
    cos_table, sin_table = unit_circle(frequencies[:, None, None] * offsets[None], length)
    return complex_times(
        real_part, imag_part, cos_table[:, :, None, None, :], sin_table[:, :, None, None, :]
    )


def row_transform(operand, frequencies, sources, period):
    cos_table, sin_table = unit_circle(frequencies[:, None] * sources[None, :], period)
    imag_matrix = -sin_table
    flipped = unit_circle(period // 2 * sources[None, :], period)[0]
    imag_matrix = jnp.where(frequencies[:, None] == 0, flipped, imag_matrix)
    return (
        jnp.dot(cos_table, operand, precision=HIGHEST_PRECISION),
        jnp.dot(imag_matrix, operand, precision=HIGHEST_PRECISION),
    )


def row_inverse(real_part, imag_part, frequencies, rows_count, period, length):
    targets = jnp.arange(rows_count, dtype=jnp.int32)
    cos_table, sin_table = unit_circle(targets[:, None] * frequencies[None, :], period)
    real_matrix = cos_table / length
    imag_matrix = -sin_table / length
    flipped = unit_circle(period // 2 * targets[:, None], period)[0]
    head_row = frequencies[None, :] == 0
    real_matrix = jnp.where(head_row, 1.0, 2.0 * cos_table) / length
    imag_matrix = jnp.where(head_row, flipped, -2.0 * sin_table) / length
    return jnp.dot(real_matrix, real_part, precision=HIGHEST_PRECISION) + jnp.dot(
        imag_matrix, imag_part, precision=HIGHEST_PRECISION
    )


def unpack_head(real_part, imag_part, first_device):
    head_row = (jnp.arange(real_part.shape[0]) == 0)[:, None, None, None, None] & first_device
    extra_row = jnp.where(first_device, imag_part[:1], 0.0)
    cleared = jnp.where(head_row, 0.0, imag_part)
    return (
        jnp.concatenate([real_part, extra_row], axis=0),
        jnp.concatenate([cleared, jnp.zeros_like(extra_row)], axis=0),
    )


def pack_head(real_part, imag_part, first_device):
    head_imag = jnp.where(first_device, real_part[-1:], imag_part[:1])
    return (real_part[:-1], jnp.concatenate([head_imag, imag_part[1:-1]], axis=0))


def spectral_middle(signal, kernel, sequences, positions, share, column_index, send_out, send_back):
    rows_count = signal.shape[0]
    period = 2 * rows_count
    column_count = lax.axis_size("col")
    length = period * column_count * positions
    local_rows = rows_count // column_count
    frequencies = jnp.arange(rows_count, dtype=jnp.int32)
    signal_sources = jnp.arange(rows_count, dtype=jnp.int32)
    kernel_index = jnp.arange(period, dtype=jnp.int32)
    kernel_sources = kernel_index % 2 * rows_count + kernel_index // 2
    signal_real, signal_imag = row_transform(signal, frequencies, signal_sources, period)
    kernel_real, kernel_imag = row_transform(kernel, frequencies, kernel_sources, period)
    moved = send_out(
        signal_real[:, None], signal_imag[:, None], kernel_real[:, None], kernel_imag[:, None]
    )
    signal_shape = (local_rows, column_count, sequences, share, positions)
    kernel_shape = (local_rows, column_count, 1, share, positions)
    signal_real = moved[0].reshape(signal_shape)
    signal_imag = moved[1].reshape(signal_shape)
    kernel_real = moved[2].reshape(kernel_shape)
    kernel_imag = moved[3].reshape(kernel_shape)
    local_freq = column_index * local_rows + jnp.arange(local_rows, dtype=jnp.int32)
    first_device = column_index == 0
    signal_real, signal_imag = unpack_head(signal_real, signal_imag, first_device)
    kernel_real, kernel_imag = unpack_head(kernel_real, kernel_imag, first_device)
    local_freq = jnp.concatenate([local_freq, jnp.full((1,), rows_count, jnp.int32)])
    signal_real, signal_imag = forward_rows(signal_real, signal_imag, local_freq, length)
    kernel_real, kernel_imag = forward_rows(kernel_real, kernel_imag, local_freq, length)
    product_real, product_imag = complex_times(signal_real, signal_imag, kernel_real, kernel_imag)
    product_real, product_imag = inverse_rows(product_real, product_imag, local_freq, length)
    product_real, product_imag = pack_head(product_real, product_imag, first_device)
    returned = send_back(product_real, product_imag)
    columns = sequences * share * positions
    return row_inverse(
        returned[0].reshape(rows_count, columns),
        returned[1].reshape(rows_count, columns),
        frequencies,
        rows_count,
        period,
        length,
    )


def local(streams, filter_taps, short_taps, skip_gain, out_weight):
    sequences, positions, channels = (streams.shape[1], streams.shape[2], streams.shape[3])
    rows_count = lax.axis_size("row")
    share = channels // rows_count
    column_index = lax.axis_index("col")
    padded = padded_2(streams, ((("row", "col"), 2),), 1)
    smoothed = (
        short_taps[:, 0][:, None, None, :] * padded[:, :, :-2]
        + short_taps[:, 1][:, None, None, :] * padded[:, :, 1:-1]
        + short_taps[:, 2][:, None, None, :] * padded[:, :, 2:]
    )
    gated = smoothed[2] * smoothed[1]
    gated_lanes = jnp.transpose(gated, (0, 2, 1))[None]
    taps_lanes = jnp.transpose(filter_taps, (0, 2, 1))[:, None]
    by_channel, kernel_channel = (
        lax.all_to_all(gated_lanes, "row", split_axis=2, concat_axis=0, tiled=True),
        lax.all_to_all(taps_lanes, "row", split_axis=2, concat_axis=0, tiled=True),
    )
    signal = by_channel.reshape(rows_count, sequences * share * positions)
    kernel = kernel_channel.reshape(2 * rows_count, share * positions)

    def send_out(part_one, part_two, part_three, part_four):
        return in_one_piece((part_one, part_two, part_three, part_four), "col", 0, 1, 2)

    def send_back(part_one, part_two):
        return in_one_piece((part_one, part_two), "col", 1, 0, 2)

    spatial = spectral_middle(
        signal, kernel, sequences, positions, share, column_index, send_out, send_back
    )
    returned = lax.all_to_all(
        spatial.reshape(rows_count, sequences, share, positions),
        "row",
        split_axis=0,
        concat_axis=2,
        tiled=True,
    )
    convolved = jnp.transpose(returned[0], (0, 2, 1))
    mixed = ((convolved + skip_gain * gated) * smoothed[0]).astype(jnp.bfloat16)
    flattened = mixed.reshape(sequences * positions, channels)
    mean_square = jnp.mean(jnp.square(flattened.astype(jnp.float32)), axis=-1, keepdims=True)
    product = jnp.dot(flattened, out_weight, preferred_element_type=jnp.float32)
    scaled = (product * lax.rsqrt(mean_square + EPSILON)).astype(jnp.bfloat16)
    return scaled.reshape(sequences, positions, out_weight.shape[1])


def solution(mesh):
    in_specs = (P(None, None, ("row", "col"), None), P(None, ("row", "col"), None), P(), P(), P())
    out_specs = P(None, ("row", "col"), None)
    return jax.shard_map(local, mesh=mesh, in_specs=in_specs, out_specs=out_specs, check_vma=False)
```

profile of v0, /device:TPU:1, one launch (start us, length us, event | category | flops | bytes accessed | tf_op | source)
XLA Modules:
  0.0 272.3 jit_solution(9572886198682673)
XLA Ops:
  0.0 0.8 fusion.340
  0.8 0.3 copy.46
  1.1 3.9 %collective-permute-start = (bf16[3,1,1,512]{2,3,1,0:T(8,128)(2,1)S(1)}, bf16[3,1,1,512]{2,3,1,0:T(8,128)(2,1)S(1)}, u32[]{:S(2)}, u32[]{:S(2)}) collective-permute-start(bf16[3,1,1,512]{2,3,1,0:T(8,128)(2,1)S(1)} %copy.46), channel_id=1, source_target_pairs={{0,1},{1,2},{2,3},{3,4},{4,5},{5,6},{6,7},{7,8},{8,9},{9,10},{10,1... | collective-permute-start | bytes 9224 | tf_op jit(solution)/shard_map/ppermute | solution.py:20
  5.0 0.3 copy.49
  5.3 6.2 %collective-permute-start.1 = (bf16[3,1,1,512]{2,3,1,0:T(8,128)(2,1)S(1)}, bf16[3,1,1,512]{2,3,1,0:T(8,128)(2,1)S(1)}, u32[]{:S(2)}, u32[]{:S(2)}) collective-permute-start(bf16[3,1,1,512]{2,3,1,0:T(8,128)(2,1)S(1)} %copy.49), channel_id=1, source_target_pairs={{1,0},{2,1},{3,2},{4,3},{5,4},{6,5},{7,6},{8,7},{9,8},{10,9},{11,1... | collective-permute-start | bytes 9224 | tf_op jit(solution)/shard_map/ppermute | solution.py:21
  11.5 0.9 fusion.341
  12.4 1.2 copy.47
  13.6 1.1 collective-permute-done
  14.8 5.7 %collective-permute-done.1 = bf16[3,1,1,512]{2,3,1,0:T(8,128)(2,1)S(1)} collective-permute-done((bf16[3,1,1,512]{2,3,1,0:T(8,128)(2,1)S(1)}, bf16[3,1,1,512]{2,3,1,0:T(8,128)(2,1)S(1)}, u32[]{:S(2)}, u32[]{:S(2)}) %collective-permute-start.1) | collective-permute-done | bytes 3104 | tf_op jit(solution)/shard_map/ppermute | solution.py:21
  20.4 1.1 multiply_add_fusion
  21.5 0.7 slice_multiply_fusion
  22.2 29.0 %all-to-all-start = ((f32[1,1,512,128]{3,1,0,2:T(1,128)}), f32[1,1,512,128]{3,1,0,2:T(1,128)S(1)}, u32[]{:S(2)}, u32[]{:S(2)}) async-start(f32[1,1,512,128]{3,1,0,2:T(1,128)} %bitcast.3), calls=%async_computation | async-start | bytes 524288 | tf_op jit(solution)/shard_map/all_to_all | solution.py:214
  51.3 1.0 copy.52
  52.3 40.3 %all-to-all-done = f32[1,1,512,128]{3,1,0,2:T(1,128)S(1)} async-done(((f32[1,1,512,128]{3,1,0,2:T(1,128)}), f32[1,1,512,128]{3,1,0,2:T(1,128)S(1)}, u32[]{:S(2)}, u32[]{:S(2)}) %all-to-all-start) | async-done | bytes 262176 | tf_op jit(solution)/shard_map/all_to_all | solution.py:214
  92.5 6.3 %all-to-all-start.1 = ((f32[2,1,512,128]{3,0,1,2:T(2,128)}), f32[2,1,512,128]{3,0,1,2:T(2,128)S(1)}, u32[]{:S(2)}, u32[]{:S(2)}) async-start(f32[2,1,512,128]{3,0,1,2:T(2,128)} %bitcast.7), calls=%async_computation.1 | async-start | bytes 1048576 | tf_op jit(solution)/shard_map/all_to_all | solution.py:215
  99.0 0.6 broadcast.912
  99.6 1.3 reduce.3
  100.9 0.5 convolution_bitcast_fusion.3
  101.4 0.5 convolution_bitcast_fusion.2
  101.9 60.7 %all-to-all-done.1 = f32[2,1,512,128]{3,0,1,2:T(2,128)S(1)} async-done(((f32[2,1,512,128]{3,0,1,2:T(2,128)}), f32[2,1,512,128]{3,0,1,2:T(2,128)S(1)}, u32[]{:S(2)}, u32[]{:S(2)}) %all-to-all-start.1) | async-done | bytes 524320 | tf_op jit(solution)/shard_map/all_to_all | solution.py:215
  162.8 0.6 convolution_bitcast_fusion.1
  163.3 0.6 convolution_bitcast_fusion
  163.9 0.1 pad_maximum_fusion
  164.0 2.0 copy.55
  166.0 7.4 %all-to-all-start.2 = ((f32[64,1,4096]{2,1,0:T(1,128)}), f32[64,1,4096]{2,1,0:T(1,128)S(1)}, u32[]{:S(2)}, u32[]{:S(2)}) async-start(f32[64,1,4096]{2,1,0:T(1,128)} %copy.55), calls=%async_computation.2 | async-start | bytes 2097152 | tf_op jit(solution)/shard_map/all_to_all | solution.py:40
  173.4 0.1 pad_add_fusion
  173.6 0.1 fusion.178
  173.6 0.1 iota_add_fusion
  173.7 0.2 fusion.126
  174.0 14.0 %all-to-all-done.2 = f32[64,1,4096]{2,1,0:T(1,128)S(1)} async-done(((f32[64,1,4096]{2,1,0:T(1,128)}), f32[64,1,4096]{2,1,0:T(1,128)S(1)}, u32[]{:S(2)}, u32[]{:S(2)}) %all-to-all-start.2) | async-done | bytes 1048608 | tf_op jit(solution)/shard_map/all_to_all | solution.py:40
  188.0 0.6 copy.152
  188.6 0.1 fusion.338
  189.0 0.2 copy_select_fusion
  189.1 0.5 fusion.57
  189.6 0.5 fusion.53
  190.3 0.5 fusion.51
  190.7 0.5 fusion.47
  191.2 0.5 fusion.6
  191.7 0.5 fusion.5
  192.2 0.5 fusion.4
  192.7 0.6 add_bitcast_fusion
  193.3 0.7 fusion.31
  193.9 0.7 fusion.27
  194.6 0.7 convolution_subtract_fusion.2
  195.3 0.7 fusion.37
  196.0 0.7 fusion.33
  196.7 0.7 convolution_subtract_fusion.4
  197.3 0.7 convolution_add_fusion.2
  198.0 0.7 multiply_subtract_fusion.2
  198.8 0.7 fusion.72
  199.4 0.9 fusion.70
  200.3 0.7 convolution_subtract_fusion.1
  201.0 0.7 multiply_subtract_fusion.1
  201.7 0.5 fusion.25
  202.2 0.5 fusion.21
  202.7 0.5 fusion.3
  203.2 0.5 multiply_subtract_fusion
  203.8 0.2 copy.75
  204.0 12.8 %all_to_all.69 = f32[4,16,2,8,128]{4,3,0,2,1:T(8,128)S(1)} all-to-all(f32[4,16,2,8,128]{4,3,0,2,1:T(8,128)S(1)} %copy.75), channel_id=1, replica_groups=mesh['row'=64,'col'=16] {'col'}, dimensions={1} | all-to-all | bytes 1048576 | tf_op jit(solution)/shard_map/all_to_all | solution.py:40
  216.9 0.5 fusion.41
  217.4 0.5 fusion.8
  218.0 52.4 %all_to_all.70 = f32[64,1,8,128]{3,2,1,0:T(8,128)S(1)} all-to-all(f32[64,1,8,128]{3,2,1,0:T(8,128)S(1)} %bitcast.273), channel_id=1, replica_groups=mesh['row'=64,'col'=16] {'row'}, dimensions={0} | all-to-all | bytes 524288 | tf_op jit(solution)/shard_map/all_to_all | solution.py:229
  270.4 0.2 multiply_reduce_fusion
  270.6 1.7 fusion.1
  (38 shorter events, 0.9 us)
Async XLA Ops:
  0.0 51.3 %copy-start.1 = (f32[2,128,512]{2,1,0:T(8,128)S(1)}, f32[2,128,512]{2,1,0:T(8,128)}, u32[]{:S(2)}) copy-start(f32[2,128,512]{2,1,0:T(8,128)} %param.6) | copy-start | bytes 1572868
  1.1 13.7 %collective-permute-start = (bf16[3,1,1,512]{2,3,1,0:T(8,128)(2,1)S(1)}, bf16[3,1,1,512]{2,3,1,0:T(8,128)(2,1)S(1)}, u32[]{:S(2)}, u32[]{:S(2)}) collective-permute-start(bf16[3,1,1,512]{2,3,1,0:T(8,128)(2,1)S(1)} %copy.46), channel_id=1, source_target_pairs={{0,1},{1,2},{2,3},{3,4},{4,5},{5,6},{6,7},{7,8},{8,9},{9,10},{10,1... | collective-permute-start | bytes 9224 | tf_op jit(solution)/shard_map/ppermute | solution.py:20
  5.3 15.1 %collective-permute-start.1 = (bf16[3,1,1,512]{2,3,1,0:T(8,128)(2,1)S(1)}, bf16[3,1,1,512]{2,3,1,0:T(8,128)(2,1)S(1)}, u32[]{:S(2)}, u32[]{:S(2)}) collective-permute-start(bf16[3,1,1,512]{2,3,1,0:T(8,128)(2,1)S(1)} %copy.49), channel_id=1, source_target_pairs={{1,0},{2,1},{3,2},{4,3},{5,4},{6,5},{7,6},{8,7},{9,8},{10,9},{11,1... | collective-permute-start | bytes 9224 | tf_op jit(solution)/shard_map/ppermute | solution.py:21
  22.2 70.3 %all-to-all-start = ((f32[1,1,512,128]{3,1,0,2:T(1,128)}), f32[1,1,512,128]{3,1,0,2:T(1,128)S(1)}, u32[]{:S(2)}, u32[]{:S(2)}) async-start(f32[1,1,512,128]{3,1,0,2:T(1,128)} %bitcast.3), calls=%async_computation | async-start | bytes 524288 | tf_op jit(solution)/shard_map/all_to_all | solution.py:214
  92.5 70.1 %all-to-all-start.1 = ((f32[2,1,512,128]{3,0,1,2:T(2,128)}), f32[2,1,512,128]{3,0,1,2:T(2,128)S(1)}, u32[]{:S(2)}, u32[]{:S(2)}) async-start(f32[2,1,512,128]{3,0,1,2:T(2,128)} %bitcast.7), calls=%async_computation.1 | async-start | bytes 1048576 | tf_op jit(solution)/shard_map/all_to_all | solution.py:215
  166.0 21.9 %all-to-all-start.2 = ((f32[64,1,4096]{2,1,0:T(1,128)}), f32[64,1,4096]{2,1,0:T(1,128)S(1)}, u32[]{:S(2)}, u32[]{:S(2)}) async-start(f32[64,1,4096]{2,1,0:T(1,128)} %copy.55), calls=%async_computation.2 | async-start | bytes 2097152 | tf_op jit(solution)/shard_map/all_to_all | solution.py:40
  203.7 66.7 %copy-start.2 = (f32[512]{0:T(512)S(1)}, f32[512]{0:T(512)}, u32[]{:S(2)}) copy-start(f32[512]{0:T(512)} %param.8) | copy-start | bytes 6148
  203.8 66.8 %copy-start = (bf16[512,4096]{1,0:T(8,128)(2,1)S(1)}, bf16[512,4096]{1,0:T(8,128)(2,1)}, u32[]{:S(2)}) copy-start(bf16[512,4096]{1,0:T(8,128)(2,1)} %param.9) | copy-start | bytes 12582916
where the time goes:
time: 273 us; the launch traced here: 272 us
  waiting for transfers between devices  122 us (45%)
  blocking collectives  65.1 us (24%)
  starting transfers between devices  52.8 us (19%)
  matrix products  19.2 us (7%)
  local copies, waits for them, and re-layouts  8.58 us (3%)
  other arithmetic  4.2 us (2%)
    all_to_all x1, waiting for transfers between devices, local(): lax.all_to_all(taps_lanes, 'row', split_axis=2, concat_axis=0, tiled=True)  60.7 us
    all_to_all x1, blocking collectives, local(): lax.all_to_all(spatial.reshape(rows_count, sequences, share, positions),...  52.4 us
    all_to_all x1, waiting for transfers between devices, local(): lax.all_to_all(gated_lanes, 'row', split_axis=2, concat_axis=0, tiled=True)  40.3 us
    all_to_all x1, starting transfers between devices, local(): lax.all_to_all(gated_lanes, 'row', split_axis=2, concat_axis=0, tiled=True)  29 us
    dot_general x24, matrix products, single(): return jnp.einsum(formula, matrix, operand, precision=HIGHEST_PRECISION)  14.2 us
    all_to_all x1, waiting for transfers between devices, in_one_piece(): lax.all_to_all(both, axis, split_axis=split_dim, concat_axis=concat_dim,...  14 us
    all_to_all x1, blocking collectives, in_one_piece(): lax.all_to_all(both, axis, split_axis=split_dim, concat_axis=concat_dim,...  12.8 us
    all_to_all x1, starting transfers between devices, in_one_piece(): lax.all_to_all(both, axis, split_axis=split_dim, concat_axis=concat_dim,...  7.36 us
  transfers between devices with their start and end apart: 5, of which 5 were waited for; matrix products, arithmetic and copies ran while one was open for 3% of the time, Pallas kernels for 0%

commit v1 on v0

v1 whole, which is shorter than its diff:
```python
import math

import jax
import jax.numpy as jnp
import numpy as np
from jax import lax
from jax.sharding import PartitionSpec as P

EPSILON = 1e-06
HIGH = lax.Precision.HIGH


def tables():
    s = np.arange(1024, dtype=np.int64)
    q = np.arange(1024, dtype=np.int64)
    j = np.arange(128, dtype=np.int64)
    ang = np.pi * ((2 * q[:, None] + 1) * s[None] % 4096) / 2048.0
    m1 = np.stack([np.cos(ang), -np.sin(ang)]).reshape(2, 2, 512, 1024).transpose(1, 0, 2, 3).reshape(2, 1024, 1024)
    ang = np.pi * ((2 * q[:, None] + 1) * j[None]) / 262144.0
    tw = np.stack([np.cos(ang), -np.sin(ang)]).reshape(2, 2, 512, 128).transpose(1, 0, 2, 3)
    ang = 2 * np.pi * (j[:, None] * j[None] % 128) / 128.0
    c, n = np.cos(ang), np.sin(ang)
    fwd = np.block([[c, -n], [n, c]])
    inv = np.block([[c, n], [-n, c]])
    return m1, tw, fwd, inv


def halo(streams):
    size = 1024
    axes = ("row", "col")
    up = [(i, i + 1) for i in range(size - 1)]
    low = lax.ppermute(streams[:, :, -1:], axes, up)
    high = lax.ppermute(streams[:, :, :1], axes, [(b, a) for a, b in up])
    return jnp.concatenate([low, streams, high], axis=2)


def local(streams, filter_taps, short_taps, skip_gain, out_weight):
    m1, tw, fwd, inv = tables()
    core = lax.axis_index("row") % 2
    m1 = jnp.asarray(m1, jnp.bfloat16)[core]
    tw = jnp.asarray(tw, jnp.float32)[core]
    fwd = jnp.asarray(fwd, jnp.float32)
    inv = jnp.asarray(inv, jnp.float32)
    padded = halo(streams)
    smoothed = (
        short_taps[:, 0][:, None, None, :] * padded[:, :, :-2]
        + short_taps[:, 1][:, None, None, :] * padded[:, :, 1:-1]
        + short_taps[:, 2][:, None, None, :] * padded[:, :, 2:]
    )[:, 0]
    gated = smoothed[2] * smoothed[1]
    data = jnp.concatenate([gated[None].astype(jnp.bfloat16), filter_taps.astype(jnp.bfloat16)], axis=0)
    data = jnp.swapaxes(data, 1, 2)
    data = lax.all_to_all(data.reshape(3, 16, 32, 128), "col", split_axis=1, concat_axis=1, tiled=True)
    data = jnp.transpose(data, (2, 0, 1, 3))
    zgroups = [[2 * z + k for z in range(32)] for k in range(2)]
    pairs = [[2 * z, 2 * z + 1] for z in range(32)]
    data = lax.all_to_all(data, "row", split_axis=0, concat_axis=0, axis_index_groups=zgroups, tiled=True)
    data = lax.all_gather(data, "row", axis_index_groups=pairs)
    data = jnp.transpose(data, (2, 1, 0, 3, 4)).reshape(3, 1024, 128)
    spec = jnp.einsum("qs,asj->aqj", m1, data, preferred_element_type=jnp.float32)
    re, im = spec[:, :512], spec[:, 512:]
    sign = (1.0 - 2.0 * (jnp.arange(512) % 2)).astype(jnp.float32)[:, None]
    hre = re[1] - sign * im[2]
    him = im[1] + sign * re[2]

    def rows(re, im):
        both = jnp.concatenate([re * tw[0] - im * tw[1], re * tw[1] + im * tw[0]], axis=1)
        out = jnp.dot(both, fwd, precision=HIGH)
        return out[:, :128], out[:, 128:]

    gre, gim = rows(re[0], im[0])
    hre, him = rows(hre, him)
    both = jnp.concatenate([gre * hre - gim * him, gre * him + gim * hre], axis=1)
    back = jnp.dot(both, inv, precision=HIGH)
    bre, bim = back[:, :128], back[:, 128:]
    both = jnp.concatenate([bre * tw[0] + bim * tw[1], bim * tw[0] - bre * tw[1]], axis=0) * (2.0 ** -17)
    hi = both.astype(jnp.bfloat16)
    lo = (both - hi.astype(jnp.float32)).astype(jnp.bfloat16)
    y = lax.dot_general(m1, jnp.concatenate([hi, lo], axis=1), (((0,), (0,)), ((), ())), preferred_element_type=jnp.float32)
    y = (y[:, :128] + y[:, 128:]).reshape(32, 2, 16, 128)
    mine = jnp.where(core == 0, y[:, 0], y[:, 1])
    other = jnp.where(core == 0, y[:, 1], y[:, 0])
    swap = [(i, i ^ 1) for i in range(64)]
    y = (mine + lax.ppermute(other, "row", swap)).astype(jnp.bfloat16)
    y = lax.all_to_all(y, "row", split_axis=0, concat_axis=0, axis_index_groups=zgroups, tiled=True)
    y = jnp.transpose(y, (1, 0, 2))
    y = lax.all_to_all(y, "col", split_axis=0, concat_axis=0, tiled=True)
    convolved = y.reshape(512, 128).T.astype(jnp.float32)
    mixed = ((convolved + skip_gain * gated) * smoothed[0]).astype(jnp.bfloat16)
    mean_square = jnp.mean(jnp.square(mixed.astype(jnp.float32)), axis=-1, keepdims=True)
    product = jnp.dot(mixed, out_weight, preferred_element_type=jnp.float32)
    return (product * lax.rsqrt(mean_square + EPSILON)).astype(jnp.bfloat16)[None]


def solution(mesh):
    in_specs = (P(None, None, ("row", "col"), None), P(None, ("row", "col"), None), P(), P(), P())
    return jax.shard_map(local, mesh=mesh, in_specs=in_specs, out_specs=P(None, ("row", "col"), None), check_vma=False)
```

time: 273 us -> 184 us (0.67)
  waiting for transfers between devices: 122 us -> 62.3 us
  matrix products: 19.2 us -> 7.81 us
  blocking collectives: 65.1 us -> 56.2 us
  starting transfers between devices: 52.8 us -> 46.7 us
    all_to_all x3 -> x1, waiting for transfers between devices: 115 us -> 54 us  [local(): lax.all_to_all(data, 'row', split_axis=0, concat_axis=0, axis_index_group...]
    all_to_all x2 -> x3, blocking collectives: 65.1 us -> 53.6 us  [the longest x1 33.3 us: local(): lax.all_to_all(y, 'row', split_axis=0, concat_axis=0, axis_index_groups=z...]
    dot_general x31 -> x9, matrix products: 19.2 us -> 7.81 us  [the longest x1 2.73 us: local(): jnp.einsum('qs,asj->aqj', m1, data, preferred_element_type=jnp.float32)]
    all_to_all x3 -> x1, starting transfers between devices: 42.7 us -> 34 us  [local(): lax.all_to_all(data, 'row', split_axis=0, concat_axis=0, axis_index_group...]
    ppermute x2 -> x3, starting transfers between devices: 10.1 us -> 12.7 us  [the longest x1 8.22 us: halo(): high = lax.ppermute(streams[:, :, :1], axes, [(b, a) for a, b in up])]
    ppermute x2 -> x3, waiting for transfers between devices: 6.79 us -> 8.29 us  [the longest x1 3.77 us: halo(): low = lax.ppermute(streams[:, :, -1:], axes, up)]
  transfers between devices with their start and end apart: 5 -> 4, of which waited for: 5 -> 4; matrix products, arithmetic and copies ran while one was open for 3% -> 2% of each run, Pallas kernels for 0% -> 0%
where the time goes in v1:
time: 184 us; the launch traced here: 182 us
  waiting for transfers between devices  62.3 us (34%)
  blocking collectives  56.2 us (31%)
  starting transfers between devices  46.7 us (25%)
  matrix products  7.81 us (4%)
  local copies, waits for them, and re-layouts  7.31 us (4%)
    all_to_all x1, waiting for transfers between devices, local(): lax.all_to_all(data, 'row', split_axis=0, concat_axis=0, axis_index_group...  54 us
    all_to_all x1, starting transfers between devices, local(): lax.all_to_all(data, 'row', split_axis=0, concat_axis=0, axis_index_group...  34 us
    all_to_all x1, blocking collectives, local(): lax.all_to_all(y, 'row', split_axis=0, concat_axis=0, axis_index_groups=z...  33.3 us
    all_to_all x1, blocking collectives, local(): lax.all_to_all(data.reshape(3, 16, 32, 128), 'col', split_axis=1, concat_...  10.9 us
    all_to_all x1, blocking collectives, local(): y = lax.all_to_all(y, 'col', split_axis=0, concat_axis=0, tiled=True)  9.43 us
    ppermute x1, starting transfers between devices, halo(): high = lax.ppermute(streams[:, :, :1], axes, [(b, a) for a, b in up])  8.22 us
    unnamed x20, local copies, waits for them, and re-layouts  4.05 us
    ppermute x1, waiting for transfers between devices, halo(): low = lax.ppermute(streams[:, :, -1:], axes, up)  3.77 us
  transfers between devices with their start and end apart: 4, of which 4 were waited for; matrix products, arithmetic and copies ran while one was open for 2% of the time, Pallas kernels for 0%

profile of v1, /device:TPU:1, one launch (start us, length us, event | category | flops | bytes accessed | tf_op | source)
XLA Modules:
  0.0 182.3 jit_solution(13137194536654462375)
XLA Ops:
  0.0 0.8 fusion.78
  0.8 0.3 copy.48
  1.0 8.2 %collective-permute-start.1 = (bf16[3,1,1,512]{2,3,1,0:T(8,128)(2,1)S(1)}, bf16[3,1,1,512]{2,3,1,0:T(8,128)(2,1)S(1)}, u32[]{:S(2)}, u32[]{:S(2)}) collective-permute-start(bf16[3,1,1,512]{2,3,1,0:T(8,128)(2,1)S(1)} %copy.48), channel_id=1, source_target_pairs={{1,0},{2,1},{3,2},{4,3},{5,4},{6,5},{7,6},{8,7},{9,8},{10,9},{11,1... | collective-permute-start | bytes 9224 | tf_op jit(solution)/shard_map/ppermute | solution.py:33
  9.3 0.3 copy.45
  9.5 1.9 %collective-permute-start = (bf16[3,1,1,512]{2,3,1,0:T(8,128)(2,1)S(1)}, bf16[3,1,1,512]{2,3,1,0:T(8,128)(2,1)S(1)}, u32[]{:S(2)}, u32[]{:S(2)}) collective-permute-start(bf16[3,1,1,512]{2,3,1,0:T(8,128)(2,1)S(1)} %copy.45), channel_id=1, source_target_pairs={{0,1},{1,2},{2,3},{3,4},{4,5},{5,6},{6,7},{7,8},{8,9},{9,10},{10,1... | collective-permute-start | bytes 9224 | tf_op jit(solution)/shard_map/ppermute | solution.py:32
  11.5 0.9 fusion.79
  12.3 1.2 copy.46
  13.6 1.2 copy.50
  14.8 3.4 %collective-permute-done.1 = bf16[3,1,1,512]{2,3,1,0:T(8,128)(2,1)S(1)} collective-permute-done((bf16[3,1,1,512]{2,3,1,0:T(8,128)(2,1)S(1)}, bf16[3,1,1,512]{2,3,1,0:T(8,128)(2,1)S(1)}, u32[]{:S(2)}, u32[]{:S(2)}) %collective-permute-start.1) | collective-permute-done | bytes 3104 | tf_op jit(solution)/shard_map/ppermute | solution.py:33
  18.2 3.8 %collective-permute-done = bf16[3,1,1,512]{2,3,1,0:T(8,128)(2,1)S(1)} collective-permute-done((bf16[3,1,1,512]{2,3,1,0:T(8,128)(2,1)S(1)}, bf16[3,1,1,512]{2,3,1,0:T(8,128)(2,1)S(1)}, u32[]{:S(2)}, u32[]{:S(2)}) %collective-permute-start) | collective-permute-done | bytes 3104 | tf_op jit(solution)/shard_map/ppermute | solution.py:32
  21.9 1.1 multiply_add_fusion
  23.1 10.9 %all_to_all.20 = bf16[3,16,32,128]{3,2,0,1:T(8,128)(2,1)S(1)} all-to-all(bf16[3,16,32,128]{3,2,0,1:T(8,128)(2,1)S(1)} %copy.51), channel_id=1, replica_groups=mesh['row'=64,'col'=16] {'col'}, dimensions={1} | all-to-all | bytes 786432 | tf_op jit(solution)/shard_map/all_to_all | solution.py:53
  34.0 0.9 copy.52
  34.9 34.0 %all-to-all-start.1 = ((bf16[32,3,16,128]{3,2,1,0:T(8,128)(2,1)}), bf16[32,3,16,128]{3,2,1,0:T(8,128)(2,1)S(1)}, u32[]{:S(2)}, u32[]{:S(2)}) async-start(bf16[32,3,16,128]{3,2,1,0:T(8,128)(2,1)} %copy.52), calls=%async_computation.1 | async-start | bytes 786432 | tf_op jit(solution)/shard_map/all_to_all | solution.py:57
  69.0 54.0 %all-to-all-done.1 = bf16[32,3,16,128]{3,2,1,0:T(8,128)(2,1)S(1)} async-done(((bf16[32,3,16,128]{3,2,1,0:T(8,128)(2,1)}), bf16[32,3,16,128]{3,2,1,0:T(8,128)(2,1)S(1)}, u32[]{:S(2)}, u32[]{:S(2)}) %all-to-all-start.1) | async-done | bytes 393248 | tf_op jit(solution)/shard_map/all_to_all | solution.py:57
  123.0 2.6 %all-gather = bf16[64,3,16,128]{3,2,1,0:T(8,128)(2,1)S(1)} all-gather(bf16[32,3,16,128]{3,2,1,0:T(8,128)(2,1)S(1)} %all-to-all-done.1), channel_id=2, replica_groups={{0,16},{32,48},{64,80},{96,112},{128,144},{160,176},{192,208},{224,240}..., dimensions={0}, use_global_device_ids=true | all-gather | bytes 1179648 | tf_op jit(solution)/shard_map/all_gather | solution.py:58
  125.6 0.1 copy.53
  125.7 0.0 copy-start
  125.8 0.0 copy-start.3
  125.8 2.7 %fusion.4 = f32[3,1024,128]{1,2,0:T(8,128)S(1)} fusion(bf16[3,1024,128]{2,1,0:T(8,128)(2,1)S(1)} %bitcast.208, bf16[2,1024,1024]{2,1,0:T(8,128)(2,1)} %constant.50.clone, s32[]{:T(128)S(6)} %select_n.43), kind=kOutput, calls=%fused_computation.7 | convolution fusion | flops 805306368 | bytes 4456452 | tf_op jit(solution)/shard_map/qs,asj->aqj/dot_general | solution.py:60
  128.5 0.0 copy-done
  128.5 0.0 copy-done.3
  128.5 0.0 copy-start.2
  128.5 0.4 fusion.22
  129.0 0.5 fusion.27
  129.4 0.0 copy-done.2
  129.4 0.0 copy-start.4
  129.5 0.0 copy-start.5
  129.5 0.5 convolution_add_fusion.1
  129.9 0.4 convolution_add_fusion.2
  130.4 0.0 copy-done.4
  130.4 0.4 fusion.48
  130.8 0.0 copy-done.5
  130.8 0.0 copy-start.7
  130.8 0.4 convolution_add_fusion
  131.3 0.1 fusion.31
  131.4 0.1 fusion.8
  131.4 1.6 copy-done.7
  133.0 0.0 copy-start.6
  133.0 0.8 fusion.2
  133.8 0.0 copy-start.1
  133.8 0.1 slice_add_fusion
  133.9 2.6 %collective-permute-start.2 = (f32[32,16,128]{2,1,0:T(8,128)S(1)}, f32[32,16,128]{2,1,0:T(8,128)S(1)}, u32[]{:S(2)}, u32[]{:S(2)}) collective-permute-start(f32[32,16,128]{2,1,0:T(8,128)S(1)} %select_bitcast_fusion), channel_id=1, source_target_pairs={{0,16},{16,0},{32,48},{48,32},{64,80},{80,64},{96,112},{112,96},{1... | collective-permute-start | bytes 786440 | tf_op jit(solution)/shard_map/ppermute | solution.py:84
  136.4 1.1 collective-permute-done.2
  137.6 0.1 fusion.44
  137.6 33.3 %all_to_all.21 = bf16[32,16,128]{2,1,0:T(8,128)(2,1)S(1)} all-to-all(bf16[32,16,128]{2,1,0:T(8,128)(2,1)S(1)} %fusion.44), channel_id=1, replica_groups={{0,32,64,96,128,160,192,224,256,288,320,352,384,416,448,480,512,544,576..., dimensions={0} | all-to-all | bytes 262144 | tf_op jit(solution)/shard_map/all_to_all | solution.py:85
  171.0 9.4 %all_to_all.22 = bf16[16,32,128]{2,1,0:T(8,128)(2,1)S(1)} all-to-all(bf16[16,32,128]{2,1,0:T(8,128)(2,1)S(1)} %bitcast.209), channel_id=1, replica_groups=mesh['row'=64,'col'=16] {'col'}, dimensions={0} | all-to-all | bytes 262144 | tf_op jit(solution)/shard_map/all_to_all | solution.py:87
  180.4 0.0 copy-done.6
  180.4 0.2 multiply_reduce_fusion
  180.6 0.0 copy-done.1
  180.6 1.7 fusion.1
  (9 shorter events, 0.2 us)
Async XLA Ops:
  1.0 17.1 %collective-permute-start.1 = (bf16[3,1,1,512]{2,3,1,0:T(8,128)(2,1)S(1)}, bf16[3,1,1,512]{2,3,1,0:T(8,128)(2,1)S(1)}, u32[]{:S(2)}, u32[]{:S(2)}) collective-permute-start(bf16[3,1,1,512]{2,3,1,0:T(8,128)(2,1)S(1)} %copy.48), channel_id=1, source_target_pairs={{1,0},{2,1},{3,2},{4,3},{5,4},{6,5},{7,6},{8,7},{9,8},{10,9},{11,1... | collective-permute-start | bytes 9224 | tf_op jit(solution)/shard_map/ppermute | solution.py:33
  9.5 12.4 %collective-permute-start = (bf16[3,1,1,512]{2,3,1,0:T(8,128)(2,1)S(1)}, bf16[3,1,1,512]{2,3,1,0:T(8,128)(2,1)S(1)}, u32[]{:S(2)}, u32[]{:S(2)}) collective-permute-start(bf16[3,1,1,512]{2,3,1,0:T(8,128)(2,1)S(1)} %copy.45), channel_id=1, source_target_pairs={{0,1},{1,2},{2,3},{3,4},{4,5},{5,6},{6,7},{7,8},{8,9},{9,10},{10,1... | collective-permute-start | bytes 9224 | tf_op jit(solution)/shard_map/ppermute | solution.py:32
  34.9 88.1 %all-to-all-start.1 = ((bf16[32,3,16,128]{3,2,1,0:T(8,128)(2,1)}), bf16[32,3,16,128]{3,2,1,0:T(8,128)(2,1)S(1)}, u32[]{:S(2)}, u32[]{:S(2)}) async-start(bf16[32,3,16,128]{3,2,1,0:T(8,128)(2,1)} %copy.52), calls=%async_computation.1 | async-start | bytes 786432 | tf_op jit(solution)/shard_map/all_to_all | solution.py:57
  125.7 2.8 %copy-start = (f32[2,2,512,128]{2,3,1,0:T(8,128)S(1)}, f32[2,2,512,128]{2,3,1,0:T(8,128)}, u32[]{:S(2)}) copy-start(f32[2,2,512,128]{2,3,1,0:T(8,128)} %constant.51.clone) | copy-start | bytes 3145732
  125.8 2.8 %copy-start.3 = (f32[128,256]{1,0:T(8,128)S(1)}, f32[128,256]{1,0:T(8,128)}, u32[]{:S(2)}) copy-start(f32[128,256]{1,0:T(8,128)} %constant.56) | copy-start | bytes 393220
  128.5 0.9 copy-start.2
  129.4 0.9 copy-start.4
  129.5 1.3 copy-start.5
  130.8 2.2 %copy-start.7 = (bf16[2,1024,1024]{2,1,0:T(8,128)(2,1)S(1)}, bf16[2,1024,1024]{2,1,0:T(8,128)(2,1)}, u32[]{:S(2)}) copy-start(bf16[2,1024,1024]{2,1,0:T(8,128)(2,1)} %constant.50.clone) | copy-start | bytes 12582916
  133.0 47.4 %copy-start.6 = (f32[512]{0:T(512)S(1)}, f32[512]{0:T(512)}, u32[]{:S(2)}) copy-start(f32[512]{0:T(512)} %param.12) | copy-start | bytes 6148
  133.8 46.8 %copy-start.1 = (bf16[512,4096]{1,0:T(8,128)(2,1)S(1)}, bf16[512,4096]{1,0:T(8,128)(2,1)}, u32[]{:S(2)}) copy-start(bf16[512,4096]{1,0:T(8,128)(2,1)} %param.13) | copy-start | bytes 12582916
  133.9 3.7 %collective-permute-start.2 = (f32[32,16,128]{2,1,0:T(8,128)S(1)}, f32[32,16,128]{2,1,0:T(8,128)S(1)}, u32[]{:S(2)}, u32[]{:S(2)}) collective-permute-start(f32[32,16,128]{2,1,0:T(8,128)S(1)} %select_bitcast_fusion), channel_id=1, source_target_pairs={{0,16},{16,0},{32,48},{48,32},{64,80},{80,64},{96,112},{112,96},{1... | collective-permute-start | bytes 786440 | tf_op jit(solution)/shard_map/ppermute | solution.py:84

commit v2 on v1

v2 whole, which is shorter than its diff:
```python
import functools

import jax
import jax.numpy as jnp
import numpy as np
from jax import lax
from jax.experimental import pallas as pl
from jax.experimental.pallas import tpu as pltpu
from jax.sharding import PartitionSpec as P

EPSILON = 1e-06
F32 = jnp.float32
BF16 = jnp.bfloat16
MESH = pl.DeviceIdType.MESH


def tables(freqs, length):
    q = np.arange(freqs, dtype=np.int64)[:, None]
    lane = np.arange(128, dtype=np.int64)[None]

    def circle(numerator, period):
        angles = 2.0 * np.pi * (numerator % period) / period
        return [np.cos(angles), -np.sin(angles)]

    twist = circle((2 * q + 1) * lane, 2 * length)
    fine = circle((2 * q + 1) * lane, 4 * freqs)
    coarse = circle((2 * q + 1) * lane * 128, 4 * freqs)
    tabs = np.stack(twist + fine + coarse).reshape(6, 2, freqs // 2, 128).transpose(1, 0, 2, 3)
    cos, sin = circle(lane.T * lane, 128)
    forward = np.block([[cos, sin], [-sin, cos]])
    back = np.block([[cos, -sin], [sin, cos]])
    pair = np.stack([forward, back])
    high = pair.astype(jnp.bfloat16)
    low = (pair - high.astype(np.float64)).astype(jnp.bfloat16)
    return tabs.astype(np.float32), np.stack([high, low], axis=1)


def dot(a, b):
    return jnp.dot(a, b, preferred_element_type=F32)


def split(x):
    high = x.astype(BF16)
    return high, (x - high.astype(F32)).astype(BF16)


def dot3(x, matrix):
    high, low = split(x)
    return dot(high, matrix[0]) + dot(low, matrix[0]) + dot(high, matrix[1])


def kernel(Z, C, taps_w, skip, streams_h, filt_h, tabs_h, dft_h, out,
           st, ft, tb, df, he, hr, sm0, sg, gt, fx, fr, gx, gr, tmpf, tmps, zf, zs, xf, xs,
           m1h, m1l, m2, hs, dc, yo, yr, zo, ro, tmpo, xo, rx,
           load, halo_s, halo_r, send, recv):
    J = 128
    CH = Z * C
    S = 2 * CH
    QH = S // 2
    QB = min(256, QH)
    GB = min(128, QH)
    SB = min(128, S)
    ZP, CP = Z + 8, C + 8
    row, col = lax.axis_index("row"), lax.axis_index("col")
    z, core = row // 2, row % 2
    mate = (z * 2 + 1 - core, col)
    block, blocks = row * C + col, 2 * Z * C
    after, before = (block + 1) % blocks, (block + blocks - 1) % blocks
    after_id, before_id = (after // C, after % C), (before // C, before % C)

    loads = [
        pltpu.make_async_copy(streams_h, st, load.at[0]),
        pltpu.make_async_copy(filt_h, ft, load.at[1]),
        pltpu.make_async_copy(tabs_h.at[core], tb, load.at[2]),
        pltpu.make_async_copy(dft_h, df, load.at[3]),
    ]
    for c in loads:
        c.start()

    def z_at(i):
        return (z + Z // 2 + ((i + 1) // 2) * (1 - 2 * (i % 2))) % Z

    def c_at(i):
        return (col + 1 + i) % C

    barrier = pltpu.get_barrier_semaphore()

    def greet_z(i, carry):
        pl.semaphore_signal(barrier, inc=1, device_id=(z_at(i) * 2 + core, col), device_id_type=MESH)
        return carry

    def greet_c(i, carry):
        pl.semaphore_signal(barrier, inc=1, device_id=(row, c_at(i)), device_id_type=MESH)
        return carry

    lax.fori_loop(0, Z - 1, greet_z, 0)
    lax.fori_loop(0, C - 1, greet_c, 0)
    for d in (mate, after_id, before_id):
        pl.semaphore_signal(barrier, inc=1, device_id=d, device_id_type=MESH)

    def to_z(src, dst, k):
        def body(i, carry):
            t = z_at(i)
            pltpu.make_async_remote_copy(
                src_ref=src.at[t], dst_ref=dst, send_sem=send.at[k], recv_sem=recv.at[k],
                device_id=(t * 2 + core, col), device_id_type=MESH).start()
            return carry
        lax.fori_loop(0, Z - 1, body, 0)

    def to_c(src, dst, k):
        def body(i, carry):
            t = c_at(i)
            pltpu.make_async_remote_copy(
                src_ref=src.at[t], dst_ref=dst, send_sem=send.at[k], recv_sem=recv.at[k],
                device_id=(row, t), device_id_type=MESH).start()
            return carry
        lax.fori_loop(0, C - 1, body, 0)

    def await_all(ref, sem):
        pltpu.make_async_copy(ref, ref, sem).wait()

    loads[1].wait()
    for h in range(2):
        fx[:, h] = ft[h].T.astype(BF16).reshape(C, Z, J)
    fr[col] = fx[col]
    loads[0].wait()
    he[...] = jnp.zeros_like(he)
    for i in range(3):
        x = st[i].astype(F32)
        he[0, i:i + 1] = x[J - 1:J]
        he[1, i:i + 1] = x[0:1]

    pl.semaphore_wait(barrier, Z - 1 + C - 1 + 3)

    halos = [
        pltpu.make_async_remote_copy(src_ref=he.at[k], dst_ref=hr.at[k], send_sem=halo_s.at[k],
                                     recv_sem=halo_r.at[k], device_id=d, device_id_type=MESH)
        for k, d in ((0, after_id), (1, before_id))
    ]
    for c in halos:
        c.start()
    to_c(fx, fr.at[col], 0)
    for c in halos:
        c.wait_recv()
    at = lax.broadcasted_iota(jnp.int32, (J, CH), 0)
    smoothed = []
    for i in range(3):
        x = st[i].astype(F32)
        low = jnp.where(block == 0, 0.0, hr[0, i:i + 1])
        high = jnp.where(block == blocks - 1, 0.0, hr[1, i:i + 1])
        low = jnp.where(at == 0, low, pltpu.roll(x, 1, 0))
        high = jnp.where(at == J - 1, high, pltpu.roll(x, J - 1, 0))
        smoothed.append(taps_w[i, 0:1] * low + taps_w[i, 1:2] * x + taps_w[i, 2:3] * high)
    gated = smoothed[2] * smoothed[1]
    gx[...] = gated.T.astype(BF16).reshape(C, Z, J)
    sm0[...] = smoothed[0]
    sg[...] = skip[...] * gated
    gr[col] = gx[col]
    to_c(gx, gr.at[col], 1)

    await_all(fr.at[pl.ds(0, C - 1)], recv.at[0])
    for h in range(2):
        for c in range(C):
            tmpf[h, c * ZP:c * ZP + Z] = fr[c, h].astype(F32)
    for h in range(2):
        for t in range(Z):
            zf[t, h] = tmpf[h, pl.ds(t, C, stride=ZP), :].astype(BF16)
    to_z(zf, xf.at[z, core], 2)
    xf[z, core] = zf[z]
    await_all(gr.at[pl.ds(0, C - 1)], recv.at[1])
    for c in range(C):
        tmps[c * ZP:c * ZP + Z] = gr[c].astype(F32)
    for t in range(Z):
        zs[t] = tmps[pl.ds(t, C, stride=ZP), :].astype(BF16)
    to_z(zs, xs.at[z, core], 3)
    xs[z, core] = zs[z]

    loads[2].wait()
    loads[3].wait()

    def build(g, carry):
        rows = pl.ds(pl.multiple_of(g * GB, GB), GB)
        fine_re, fine_im = tb[2, rows, 0:SB], tb[3, rows, 0:SB]
        for a in range(S // SB):
            coarse_re, coarse_im = tb[4, rows, a:a + 1], tb[5, rows, a:a + 1]
            parts = (coarse_re * fine_re - coarse_im * fine_im, coarse_re * fine_im + coarse_im * fine_re)
            for k, part in enumerate(parts):
                high, low = split(part)
                per = QB // GB
                where = pl.ds(pl.multiple_of((g % per) * GB, GB) + k * QB, GB)
                m1h[g // per, where, a * SB:(a + 1) * SB] = high
                m1l[g // per, where, a * SB:(a + 1) * SB] = low
                flipped = part.T.astype(BF16)
                for n in range(SB // C):
                    tile = a * (SB // C) + n
                    m2[tile % 2, (tile // 2) * C:(tile // 2 + 1) * C, pl.ds(pl.multiple_of(g * GB, GB) + k * QH, GB)] = (
                        flipped[n * C:(n + 1) * C])
        return carry

    lax.fori_loop(0, QH // GB, build, 0)

    def to_mate(src, dst, k):
        pltpu.make_async_remote_copy(
            src_ref=src, dst_ref=dst, send_sem=send.at[k], recv_sem=recv.at[k],
            device_id=mate, device_id_type=MESH).start()

    def twisted(re, im, rows, sign):
        tw_re, tw_im = tb[0, rows], sign * tb[1, rows]
        return re * tw_re - im * tw_im, re * tw_im + im * tw_re

    await_all(xf.at[pl.ds(0, Z - 1), 0], recv.at[2])
    to_mate(xf.at[:, core], xf.at[:, core], 4)
    await_all(xf.at[:, 0], recv.at[4])

    def filter_rows(b, carry):
        rows = pl.ds(pl.multiple_of(b * QB, QB), QB)
        taps = jnp.concatenate([xf[:, :, h].reshape(S, J) for h in range(2)], axis=1)
        p = dot(m1h[b], taps) + dot(m1l[b], taps)
        sign = 1.0 - 2.0 * (lax.broadcasted_iota(jnp.int32, (QB, J), 0) % 2).astype(F32)
        re = p[:QB, :J] - sign * p[QB:, J:]
        im = p[QB:, :J] + sign * p[:QB, J:]
        hs[rows] = dot3(jnp.concatenate(twisted(re, im, rows, 1.0), axis=1), df[0])
        return carry

    lax.fori_loop(0, QH // QB, filter_rows, 0)

    await_all(xs.at[pl.ds(0, Z - 1), 0], recv.at[3])
    to_mate(xs.at[:, core], xs.at[:, core], 5)
    await_all(xs.at[:, 0], recv.at[5])

    def signal_rows(b, carry):
        rows = pl.ds(pl.multiple_of(b * QB, QB), QB)
        p = dot(m1h[b], xs[...].reshape(S, J))
        g = dot3(jnp.concatenate(twisted(p[:QB], p[QB:], rows, 1.0), axis=1), df[0])
        h = hs[rows]
        gre, gim, hre, him = g[:, :J], g[:, J:], h[:, :J], h[:, J:]
        y = dot3(jnp.concatenate([gre * hre - gim * him, gre * him + gim * hre], axis=1), df[1])
        parts = twisted(y[:, :J], y[:, J:], rows, -1.0)
        for k, part in enumerate(parts):
            high, low = split(part * (1.0 / (S * J)))
            where = pl.ds(pl.multiple_of(b * QB, QB) + k * QH, QB)
            dc[where, 0:J] = high
            dc[where, J:2 * J] = low
        return carry

    lax.fori_loop(0, QH // QB, signal_rows, 0)
    other = dot(m2[1 - core], dc[...])
    yo[...] = (other[:, :J] + other[:, J:]).reshape(Z, C, J)
    to_mate(yo, yr, 6)
    own = dot(m2[core], dc[...])
    own = (own[:, :J] + own[:, J:]).reshape(Z, C, J)
    await_all(yr, recv.at[6])
    zo[...] = (own + yr[...]).astype(BF16)
    to_z(zo, ro.at[z], 7)
    ro[z] = zo[z]
    await_all(ro.at[pl.ds(0, Z - 1)], recv.at[7])
    for t in range(Z):
        tmpo[t * CP:t * CP + C] = ro[t].astype(F32)
    for c in range(C):
        xo[c] = tmpo[pl.ds(c, Z, stride=CP), :].astype(BF16)
    to_c(xo, rx.at[col], 8)
    rx[col] = xo[col]
    await_all(rx.at[pl.ds(0, C - 1)], recv.at[8])
    convolved = rx[...].reshape(CH, J).astype(F32).T
    out[...] = ((convolved + sg[...]) * sm0[...]).astype(BF16)

    for c in halos:
        c.wait_send()
    for ref, k in ((fx.at[pl.ds(0, C - 1)], 0), (gx.at[pl.ds(0, C - 1)], 1), (zf.at[pl.ds(0, Z - 1)], 2),
                   (zs.at[pl.ds(0, Z - 1)], 3), (xf.at[:, 0], 4), (xs.at[:, 0], 5), (yo, 6),
                   (zo.at[pl.ds(0, Z - 1)], 7), (xo.at[pl.ds(0, C - 1)], 8)):
        await_all(ref, send.at[k])


def convolve(Z, C, streams, filter_taps, short_taps, skip_gain):
    J, CH = 128, Z * C
    S = 2 * CH
    QH = S // 2
    QB = min(256, QH)
    tabs, dfts = tables(S, 2 * S * J)
    vmem = pltpu.VMEM
    scratch = [
        vmem((3, J, CH), BF16),
        vmem((2, J, CH), F32),
        vmem((6, QH, 128), F32),
        vmem((2, 2, 2 * J, 2 * J), BF16),
        vmem((2, 8, CH), F32),
        vmem((2, 8, CH), F32),
        vmem((J, CH), F32),
        vmem((J, CH), F32),
        vmem((8, 128), F32),
        vmem((C, 2, Z, J), BF16),
        vmem((C, 2, Z, J), BF16),
        vmem((C, Z, J), BF16),
        vmem((C, Z, J), BF16),
        vmem((2, C * (Z + 8), J), F32),
        vmem((C * (Z + 8), J), F32),
        vmem((Z, 2, C, J), BF16),
        vmem((Z, C, J), BF16),
        vmem((Z, 2, 2, C, J), BF16),
        vmem((Z, 2, C, J), BF16),
        vmem((QH // QB, 2 * QB, S), BF16),
        vmem((QH // QB, 2 * QB, S), BF16),
        vmem((2, S // 2, 2 * QH), BF16),
        vmem((QH, 2 * J), F32),
        vmem((2 * QH, 2 * J), BF16),
        vmem((Z, C, J), F32),
        vmem((Z, C, J), F32),
        vmem((Z, C, J), BF16),
        vmem((Z, C, J), BF16),
        vmem((Z * (C + 8), J), F32),
        vmem((C, Z, J), BF16),
        vmem((C, Z, J), BF16),
        pltpu.SemaphoreType.DMA((4,)),
        pltpu.SemaphoreType.DMA((2,)),
        pltpu.SemaphoreType.DMA((2,)),
        pltpu.SemaphoreType.DMA((9,)),
        pltpu.SemaphoreType.DMA((9,)),
    ]
    inside, outside = pl.BlockSpec(memory_space=pltpu.VMEM), pl.BlockSpec(memory_space=pl.ANY)
    return pl.pallas_call(
        functools.partial(kernel, Z, C),
        out_shape=jax.ShapeDtypeStruct((J, CH), BF16),
        in_specs=[inside, inside, outside, outside, outside, outside],
        out_specs=inside,
        scratch_shapes=scratch,
        compiler_params=pltpu.CompilerParams(collective_id=0, has_side_effects=True),
        name="conv",
    )(short_taps, skip_gain[None], streams[:, 0], filter_taps, jnp.asarray(tabs), jnp.asarray(dfts))


def local(streams, filter_taps, short_taps, skip_gain, out_weight):
    rows, cols = lax.axis_size("row"), lax.axis_size("col")
    mixed = convolve(rows // 2, cols, streams, filter_taps, short_taps, skip_gain)
    mean_square = jnp.mean(jnp.square(mixed.astype(F32)), axis=-1, keepdims=True)
    product = jnp.dot(mixed, out_weight, preferred_element_type=F32)
    return (product * lax.rsqrt(mean_square + EPSILON)).astype(BF16)[None]


def solution(mesh):
    in_specs = (P(None, None, ("row", "col"), None), P(None, ("row", "col"), None), P(), P(), P())
    return jax.shard_map(local, mesh=mesh, in_specs=in_specs, out_specs=P(None, ("row", "col"), None), check_vma=False)
```

time: 184 us -> 106 us (0.58)
  Pallas kernels: 0 us -> 99.6 us
  waiting for transfers between devices: 62.3 us -> 0 us
  blocking collectives: 56.2 us -> 0 us
  starting transfers between devices: 46.7 us -> 0 us
  local copies, waits for them, and re-layouts: 7.31 us -> 0 us
  matrix products: 7.81 us -> 3.97 us
    pallas_call x0 -> x1, Pallas kernels: none -> 99.6 us  [convolve(): pl.pallas_call(functools.partial(kernel, Z, C), out_shape=jax.ShapeDtypeS...]
    all_to_all x1 -> x0, waiting for transfers between devices: 54 us -> none  [local(): lax.all_to_all(data, 'row', split_axis=0, concat_axis=0, axis_index_group...]
    all_to_all x3 -> x0, blocking collectives: 53.6 us -> none  [the longest x1 33.3 us: local(): lax.all_to_all(y, 'row', split_axis=0, concat_axis=0, axis_index_groups=z...]
    all_to_all x1 -> x0, starting transfers between devices: 34 us -> none  [local(): lax.all_to_all(data, 'row', split_axis=0, concat_axis=0, axis_index_group...]
    ppermute x3 -> x0, starting transfers between devices: 12.7 us -> none  [the longest x1 8.22 us: halo(): high = lax.ppermute(streams[:, :, :1], axes, [(b, a) for a, b in up])]
    ppermute x3 -> x0, waiting for transfers between devices: 8.29 us -> none  [the longest x1 3.77 us: halo(): low = lax.ppermute(streams[:, :, -1:], axes, up)]
    unnamed x20 -> x0, local copies, waits for them, and re-layouts: 4.05 us -> none
    dot_general x9 -> x1, matrix products: 7.81 us -> 3.97 us  [local(): product = jnp.dot(mixed, out_weight, preferred_element_type=F32)]
  transfers between devices with their start and end apart: 4 -> 0, of which waited for: 4 -> 0; matrix products, arithmetic and copies ran while one was open for 2% -> 0% of each run, Pallas kernels for 0% -> 0%
where the time goes in v2:
time: 106 us; the launch traced here: 105 us
  Pallas kernels  99.6 us (94%)
  matrix products  3.97 us (4%)
    pallas_call x1, Pallas kernels, convolve(): pl.pallas_call(functools.partial(kernel, Z, C), out_shape=jax.ShapeDtypeS...  99.6 us
    dot_general x1, matrix products, local(): product = jnp.dot(mixed, out_weight, preferred_element_type=F32)  3.97 us

profile of v2, /device:TPU:1, one launch (start us, length us, event | category | flops | bytes accessed | tf_op | source)
XLA Modules:
  0.0 104.6 jit_solution(12530667059253241395)
XLA Ops:
  0.0 99.6 %conv.1 = bf16[128,512]{1,0:T(8,128)(2,1)} custom-call(f32[3,3,512]{2,1,0:T(4,128)} %taps_w.1, f32[1,512]{1,0:T(1,128)} %bitcast.7, bf16[3,128,512]{2,1,0:T(8,128)(2,1)} %bitcast.6, f32[2,128,512]{2,1,0:T(8,128)} %filt_h.1, f32[2,6,512,128]{3,2,1,0:T(8,128)} %constant.11.clone.tabs_h, bf16[2,2,256,256]{3,2,1,0:T(8,128)(2,1)} %constant.12.clone.dft_h), custom_call_target="tpu_custom_call" | custom-call | tf_op jit(solution)/shard_map/conv/pallas_call | solution.py:321
  99.6 1.0 multiply_reduce_fusion
  100.6 4.0 %fusion.1 = bf16[1,128,4096]{2,1,0:T(8,128)(2,1)} fusion(bf16[128,512]{1,0:T(8,128)(2,1)} %conv.1, bf16[512,4096]{1,0:T(8,128)(2,1)} %param.11, f32[128]{0:T(128)S(1)} %add_rsqrt_fusion), kind=kOutput, calls=%fused_computation.2 | convolution fusion | flops 537919488 | bytes 5374464 | tf_op jit(solution)/shard_map/dot_general | solution.py:336
  (1 shorter events, 0.0 us)

commit v3 on v2

--- a/solution.py
+++ b/solution.py
@@ -49,10 +49,10 @@
     return dot(high, matrix[0]) + dot(low, matrix[0]) + dot(high, matrix[1])
 
 
-def kernel(Z, C, taps_w, skip, streams_h, filt_h, tabs_h, dft_h, out,
-           st, ft, tb, df, he, hr, sm0, sg, gt, fx, fr, gx, gr, tmpf, tmps, zf, zs, xf, xs,
+def kernel(Z, C, taps_h, skip_h, streams_h, filt_h, tabs_h, dft_h, out, scale,
+           taps_w, skip, st, ft, tb, df, he, hr, sm0, sg, fx, fr, gx, gr, tmpf, tmps, zf, zs, xf, xs,
            m1h, m1l, m2, hs, dc, yo, yr, zo, ro, tmpo, xo, rx,
-           load, halo_s, halo_r, send, recv):
+           load, halo_s, halo_r, send, recv, reach):
     J = 128
     CH = Z * C
     S = 2 * CH
@@ -73,6 +73,8 @@
         pltpu.make_async_copy(filt_h, ft, load.at[1]),
         pltpu.make_async_copy(tabs_h.at[core], tb, load.at[2]),
         pltpu.make_async_copy(dft_h, df, load.at[3]),
+        pltpu.make_async_copy(taps_h, taps_w, load.at[4]),
+        pltpu.make_async_copy(skip_h, skip, load.at[5]),
     ]
     for c in loads:
         c.start()
@@ -85,27 +87,40 @@
 
     barrier = pltpu.get_barrier_semaphore()
 
-    def greet_z(i, carry):
-        pl.semaphore_signal(barrier, inc=1, device_id=(z_at(i) * 2 + core, col), device_id_type=MESH)
-        return carry
-
     def greet_c(i, carry):
         pl.semaphore_signal(barrier, inc=1, device_id=(row, c_at(i)), device_id_type=MESH)
         return carry
 
-    lax.fori_loop(0, Z - 1, greet_z, 0)
+    def along_z(k):
+        return ((z + k) % Z) * 2 + core, col
+
+    for d in (along_z(1), along_z(Z - 1), mate, after_id, before_id):
+        pl.semaphore_signal(barrier, inc=1, device_id=d, device_id_type=MESH)
     lax.fori_loop(0, C - 1, greet_c, 0)
-    for d in (mate, after_id, before_id):
-        pl.semaphore_signal(barrier, inc=1, device_id=d, device_id_type=MESH)
-
-    def to_z(src, dst, k):
+
+    def tell(k):
+        if 2 ** k < Z // 2:
+            for d in (along_z(2 ** k), along_z(Z - 2 ** k)):
+                pl.semaphore_signal(reach.at[k], inc=1, device_id=d, device_id_type=MESH)
+
+    def hear(k):
+        if 2 ** k < Z // 2:
+            pl.semaphore_wait(reach.at[k], 2)
+
+    def to_z(src, dst, k, parity=None):
+        def pick(i):
+            if parity is None:
+                return z_at(i)
+            odd, sign = (z + parity) % 2, 1 - 2 * (i % 2)
+            return (z + Z // 2 + sign * (odd * (1 + 2 * (i // 2)) + (1 - odd) * 2 * ((i + 1) // 2))) % Z
+
         def body(i, carry):
-            t = z_at(i)
+            t = pick(i)
             pltpu.make_async_remote_copy(
                 src_ref=src.at[t], dst_ref=dst, send_sem=send.at[k], recv_sem=recv.at[k],
                 device_id=(t * 2 + core, col), device_id_type=MESH).start()
             return carry
-        lax.fori_loop(0, Z - 1, body, 0)
+        lax.fori_loop(0, Z - 1 if parity is None else Z // 2 - 1 + (z + parity) % 2, body, 0)
 
     def to_c(src, dst, k):
         def body(i, carry):
@@ -130,7 +145,8 @@
         he[0, i:i + 1] = x[J - 1:J]
         he[1, i:i + 1] = x[0:1]
 
-    pl.semaphore_wait(barrier, Z - 1 + C - 1 + 3)
+    pl.semaphore_wait(barrier, C - 1 + 5)
+    tell(0)
 
     halos = [
         pltpu.make_async_remote_copy(src_ref=he.at[k], dst_ref=hr.at[k], send_sem=halo_s.at[k],
@@ -140,6 +156,12 @@
     for c in halos:
         c.start()
     to_c(fx, fr.at[col], 0)
+    loads[4].wait()
+    loads[5].wait()
+    hear(0)
+    tell(1)
+    hear(1)
+    tell(2)
     for c in halos:
         c.wait_recv()
     at = lax.broadcasted_iota(jnp.int32, (J, CH), 0)
@@ -157,6 +179,8 @@
     sg[...] = skip[...] * gated
     gr[col] = gx[col]
     to_c(gx, gr.at[col], 1)
+    hear(2)
+    tell(3)
 
     await_all(fr.at[pl.ds(0, C - 1)], recv.at[0])
     for h in range(2):
@@ -165,14 +189,17 @@
     for h in range(2):
         for t in range(Z):
             zf[t, h] = tmpf[h, pl.ds(t, C, stride=ZP), :].astype(BF16)
-    to_z(zf, xf.at[z, core], 2)
+    hear(3)
+    to_z(zf, xf.at[z, core], 2, 0)
     xf[z, core] = zf[z]
     await_all(gr.at[pl.ds(0, C - 1)], recv.at[1])
     for c in range(C):
         tmps[c * ZP:c * ZP + Z] = gr[c].astype(F32)
     for t in range(Z):
         zs[t] = tmps[pl.ds(t, C, stride=ZP), :].astype(BF16)
-    to_z(zs, xs.at[z, core], 3)
+    to_z(zs, xs.at[z, core], 3, 0)
+    to_z(zf, xf.at[z, core], 2, 1)
+    to_z(zs, xs.at[z, core], 3, 1)
     xs[z, core] = zs[z]
 
     loads[2].wait()
@@ -262,7 +289,10 @@
     rx[col] = xo[col]
     await_all(rx.at[pl.ds(0, C - 1)], recv.at[8])
     convolved = rx[...].reshape(CH, J).astype(F32).T
-    out[...] = ((convolved + sg[...]) * sm0[...]).astype(BF16)
+    mixed = ((convolved + sg[...]) * sm0[...]).astype(BF16)
+    out[...] = mixed
+    mean_square = jnp.mean(jnp.square(mixed.astype(F32)), axis=-1, keepdims=True)
+    scale[...] = jnp.broadcast_to(lax.rsqrt(mean_square + EPSILON), (J, 128))
 
     for c in halos:
         c.wait_send()
@@ -280,6 +310,8 @@
     tabs, dfts = tables(S, 2 * S * J)
     vmem = pltpu.VMEM
     scratch = [
+        vmem((3, 3, CH), F32),
+        vmem((1, CH), F32),
         vmem((3, J, CH), BF16),
         vmem((2, J, CH), F32),
         vmem((6, QH, 128), F32),
@@ -288,7 +320,6 @@
         vmem((2, 8, CH), F32),
         vmem((J, CH), F32),
         vmem((J, CH), F32),
-        vmem((8, 128), F32),
         vmem((C, 2, Z, J), BF16),
         vmem((C, 2, Z, J), BF16),
         vmem((C, Z, J), BF16),
@@ -311,30 +342,30 @@
         vmem((Z * (C + 8), J), F32),
         vmem((C, Z, J), BF16),
         vmem((C, Z, J), BF16),
-        pltpu.SemaphoreType.DMA((4,)),
+        pltpu.SemaphoreType.DMA((6,)),
         pltpu.SemaphoreType.DMA((2,)),
         pltpu.SemaphoreType.DMA((2,)),
         pltpu.SemaphoreType.DMA((9,)),
         pltpu.SemaphoreType.DMA((9,)),
+        pltpu.SemaphoreType.REGULAR((4,)),
     ]
-    inside, outside = pl.BlockSpec(memory_space=pltpu.VMEM), pl.BlockSpec(memory_space=pl.ANY)
+    inside, outside = pl.BlockSpec(memory_space=pltpu.VMEM), pl.BlockSpec(memory_space=pltpu.HBM)
     return pl.pallas_call(
         functools.partial(kernel, Z, C),
-        out_shape=jax.ShapeDtypeStruct((J, CH), BF16),
-        in_specs=[inside, inside, outside, outside, outside, outside],
-        out_specs=inside,
+        out_shape=[jax.ShapeDtypeStruct((J, CH), BF16), jax.ShapeDtypeStruct((J, 128), F32)],
+        in_specs=[outside, outside, outside, outside, outside, outside],
+        out_specs=[inside, inside],
         scratch_shapes=scratch,
-        compiler_params=pltpu.CompilerParams(collective_id=0, has_side_effects=True),
+        compiler_params=pltpu.CompilerParams(collective_id=0, has_side_effects=True, vmem_limit_bytes=58 * 2**20),
         name="conv",
     )(short_taps, skip_gain[None], streams[:, 0], filter_taps, jnp.asarray(tabs), jnp.asarray(dfts))
 
 
 def local(streams, filter_taps, short_taps, skip_gain, out_weight):
     rows, cols = lax.axis_size("row"), lax.axis_size("col")
-    mixed = convolve(rows // 2, cols, streams, filter_taps, short_taps, skip_gain)
-    mean_square = jnp.mean(jnp.square(mixed.astype(F32)), axis=-1, keepdims=True)
+    mixed, scale = convolve(rows // 2, cols, streams, filter_taps, short_taps, skip_gain)
     product = jnp.dot(mixed, out_weight, preferred_element_type=F32)
-    return (product * lax.rsqrt(mean_square + EPSILON)).astype(BF16)[None]
+    return (product * scale[:, :1]).astype(BF16)[None]
 
 
 def solution(mesh):

time: 106 us -> 103 us (0.972)
  matrix products: 3.97 us -> 2.6 us
  Pallas kernels: 99.6 us -> 98.3 us
    dot_general x1, matrix products: 3.97 us -> 2.6 us  [local(): product = jnp.dot(mixed, out_weight, preferred_element_type=F32)]
    pallas_call x1, Pallas kernels: 99.6 us -> 98.3 us  [convolve(): pl.pallas_call(functools.partial(kernel, Z, C), out_shape=[jax.ShapeDtype...]
where the time goes in v3:
time: 103 us; the launch traced here: 102 us
  Pallas kernels  98.3 us (95%)
  matrix products  2.6 us (3%)
    pallas_call x1, Pallas kernels, convolve(): pl.pallas_call(functools.partial(kernel, Z, C), out_shape=[jax.ShapeDtype...  98.3 us
    dot_general x1, matrix products, local(): product = jnp.dot(mixed, out_weight, preferred_element_type=F32)  2.6 us

profile of v3, /device:TPU:1, one launch (start us, length us, event | category | flops | bytes accessed | tf_op | source)
XLA Modules:
  0.0 101.8 jit_solution(17669585333062289052)
XLA Ops:
  0.0 0.0 copy-start
  0.0 98.3 %conv.1 = (bf16[128,512]{1,0:T(8,128)(2,1)}, f32[128,128]{1,0:T(8,128)}) custom-call(f32[3,3,512]{2,1,0:T(4,128)} %taps_h.1, f32[1,512]{1,0:T(1,128)} %bitcast.7, bf16[3,128,512]{2,1,0:T(8,128)(2,1)} %bitcast.6, f32[2,128,512]{2,1,0:T(8,128)} %filt_h.1, f32[2,6,512,128]{3,2,1,0:T(8,128)} %constant.4.clone.tabs_h, bf16[2,2,256,256]{3,2,1,0:T(8,128)(2,1)} %constant.5.clone.dft_h), custom_call_target="tpu_custom_call" | custom-call | tf_op jit(solution)/shard_map/conv/pallas_call | solution.py:353
  98.3 0.9 slice_reduce_fusion
  99.2 0.0 copy-done
  99.2 2.6 %fusion.1 = bf16[1,128,4096]{2,1,0:T(8,128)(2,1)} fusion(bf16[128,512]{1,0:T(8,128)(2,1)} %get-tuple-element.7, bf16[512,4096]{1,0:T(8,128)(2,1)S(1)} %copy-done, f32[128]{0:T(128)S(1)} %slice_reduce_fusion), kind=kOutput, calls=%fused_computation.2 | convolution fusion | flops 537919488 | bytes 5374464 | tf_op jit(solution)/shard_map/dot_general | solution.py:367
Async XLA Ops:
  0.0 99.2 %copy-start = (bf16[512,4096]{1,0:T(8,128)(2,1)S(1)}, bf16[512,4096]{1,0:T(8,128)(2,1)}, u32[]{:S(2)}) copy-start(bf16[512,4096]{1,0:T(8,128)(2,1)} %param.11) | copy-start | bytes 12582916

commit v4 on v3

--- a/solution.py
+++ b/solution.py
@@ -76,14 +76,11 @@
         pltpu.make_async_copy(taps_h, taps_w, load.at[4]),
         pltpu.make_async_copy(skip_h, skip, load.at[5]),
     ]
-    for c in loads:
-        c.start()
-
     def z_at(i):
         return (z + Z // 2 + ((i + 1) // 2) * (1 - 2 * (i % 2))) % Z
 
     def c_at(i):
-        return (col + 1 + i) % C
+        return (col + 1 + (i + 5 * C // 8 - 1) % (C - 1)) % C
 
     barrier = pltpu.get_barrier_semaphore()
 
@@ -96,7 +93,11 @@
 
     for d in (along_z(1), along_z(Z - 1), mate, after_id, before_id):
         pl.semaphore_signal(barrier, inc=1, device_id=d, device_id_type=MESH)
-    lax.fori_loop(0, C - 1, greet_c, 0)
+    for k in (1, 0):
+        loads[k].start()
+    lax.fori_loop(0, C - 1, greet_c, 0, unroll=True)
+    for c in loads[2:]:
+        c.start()
 
     def tell(k):
         if 2 ** k < Z // 2:
@@ -107,20 +108,33 @@
         if 2 ** k < Z // 2:
             pl.semaphore_wait(reach.at[k], 2)
 
-    def to_z(src, dst, k, parity=None):
-        def pick(i):
-            if parity is None:
-                return z_at(i)
-            odd, sign = (z + parity) % 2, 1 - 2 * (i % 2)
-            return (z + Z // 2 + sign * (odd * (1 + 2 * (i // 2)) + (1 - odd) * 2 * ((i + 1) // 2))) % Z
-
+    def to_z(src, dst, k, choose=None):
         def body(i, carry):
-            t = pick(i)
-            pltpu.make_async_remote_copy(
-                src_ref=src.at[t], dst_ref=dst, send_sem=send.at[k], recv_sem=recv.at[k],
-                device_id=(t * 2 + core, col), device_id_type=MESH).start()
+            t = z_at(i)
+
+            def go():
+                pltpu.make_async_remote_copy(
+                    src_ref=src.at[t], dst_ref=dst, send_sem=send.at[k], recv_sem=recv.at[k],
+                    device_id=(t * 2 + core, col), device_id_type=MESH).start()
+
+            if choose is None:
+                go()
+            else:
+                pl.when(choose((i + 1) // 2, t))(go)
             return carry
-        lax.fori_loop(0, Z - 1 if parity is None else Z // 2 - 1 + (z + parity) % 2, body, 0)
+        lax.fori_loop(0, Z - 1, body, 0)
+
+    def near_first(n, t):
+        return n >= Z // 4
+
+    def far_first(n, t):
+        return n < Z // 4
+
+    def first(n, t):
+        return t % 4 != 3
+
+    def last(n, t):
+        return t % 4 == 3
 
     def to_c(src, dst, k):
         def body(i, carry):
@@ -129,7 +143,7 @@
                 src_ref=src.at[t], dst_ref=dst, send_sem=send.at[k], recv_sem=recv.at[k],
                 device_id=(row, t), device_id_type=MESH).start()
             return carry
-        lax.fori_loop(0, C - 1, body, 0)
+        lax.fori_loop(0, C - 1, body, 0, unroll=True)
 
     def await_all(ref, sem):
         pltpu.make_async_copy(ref, ref, sem).wait()
@@ -189,17 +203,17 @@
     for h in range(2):
         for t in range(Z):
             zf[t, h] = tmpf[h, pl.ds(t, C, stride=ZP), :].astype(BF16)
-    hear(3)
-    to_z(zf, xf.at[z, core], 2, 0)
+    to_z(zf, xf.at[z, core], 2, near_first)
     xf[z, core] = zf[z]
     await_all(gr.at[pl.ds(0, C - 1)], recv.at[1])
     for c in range(C):
         tmps[c * ZP:c * ZP + Z] = gr[c].astype(F32)
     for t in range(Z):
         zs[t] = tmps[pl.ds(t, C, stride=ZP), :].astype(BF16)
-    to_z(zs, xs.at[z, core], 3, 0)
-    to_z(zf, xf.at[z, core], 2, 1)
-    to_z(zs, xs.at[z, core], 3, 1)
+    hear(3)
+    to_z(zf, xf.at[z, core], 2, far_first)
+    for k in range(4):
+        to_z(zs, xs.at[z, core], 3, lambda n, t, k=k: t % 4 == k)
     xs[z, core] = zs[z]
 
     loads[2].wait()
@@ -270,7 +284,7 @@
             dc[where, J:2 * J] = low
         return carry
 
-    lax.fori_loop(0, QH // QB, signal_rows, 0)
+    lax.fori_loop(0, QH // QB, signal_rows, 0, unroll=True)
     other = dot(m2[1 - core], dc[...])
     yo[...] = (other[:, :J] + other[:, J:]).reshape(Z, C, J)
     to_mate(yo, yr, 6)
@@ -292,7 +306,7 @@
     mixed = ((convolved + sg[...]) * sm0[...]).astype(BF16)
     out[...] = mixed
     mean_square = jnp.mean(jnp.square(mixed.astype(F32)), axis=-1, keepdims=True)
-    scale[...] = jnp.broadcast_to(lax.rsqrt(mean_square + EPSILON), (J, 128))
+    scale[...] = jnp.broadcast_to(lax.rsqrt(mean_square + EPSILON), (J, J)).T[0:1]
 
     for c in halos:
         c.wait_send()
@@ -352,11 +366,11 @@
     inside, outside = pl.BlockSpec(memory_space=pltpu.VMEM), pl.BlockSpec(memory_space=pltpu.HBM)
     return pl.pallas_call(
         functools.partial(kernel, Z, C),
-        out_shape=[jax.ShapeDtypeStruct((J, CH), BF16), jax.ShapeDtypeStruct((J, 128), F32)],
-        in_specs=[outside, outside, outside, outside, outside, outside],
+        out_shape=[jax.ShapeDtypeStruct((J, CH), BF16), jax.ShapeDtypeStruct((1, J), F32)],
+        in_specs=[outside] * 6,
         out_specs=[inside, inside],
         scratch_shapes=scratch,
-        compiler_params=pltpu.CompilerParams(collective_id=0, has_side_effects=True, vmem_limit_bytes=58 * 2**20),
+        compiler_params=pltpu.CompilerParams(collective_id=0, has_side_effects=True, vmem_limit_bytes=429 * 2**17),
         name="conv",
     )(short_taps, skip_gain[None], streams[:, 0], filter_taps, jnp.asarray(tabs), jnp.asarray(dfts))
 
@@ -365,7 +379,7 @@
     rows, cols = lax.axis_size("row"), lax.axis_size("col")
     mixed, scale = convolve(rows // 2, cols, streams, filter_taps, short_taps, skip_gain)
     product = jnp.dot(mixed, out_weight, preferred_element_type=F32)
-    return (product * scale[:, :1]).astype(BF16)[None]
+    return (product * scale[0][:, None]).astype(BF16)[None]
 
 
 def solution(mesh):

time: 103 us -> 97.9 us (0.950)
  Pallas kernels: 98.3 us -> 94.5 us
    pallas_call x1, Pallas kernels: 98.3 us -> 94.5 us  [convolve(): pl.pallas_call(functools.partial(kernel, Z, C), out_shape=[jax.ShapeDtype...]
    unnamed x2 -> x6, local copies, waits for them, and re-layouts: 0.01 us -> 1.42 us
where the time goes in v4:
time: 97.9 us; the launch traced here: 97.7 us
  Pallas kernels  94.5 us (97%)
  matrix products  1.74 us (2%)
  local copies, waits for them, and re-layouts  1.42 us (1%)
    pallas_call x1, Pallas kernels, convolve(): pl.pallas_call(functools.partial(kernel, Z, C), out_shape=[jax.ShapeDtype...  94.5 us

profile of v4, /device:TPU:1, one launch (start us, length us, event | category | flops | bytes accessed | tf_op | source)
XLA Modules:
  0.0 97.7 jit_solution(4130549326827213255)
XLA Ops:
  0.0 0.0 copy-start
  0.0 0.7 copy-done
  0.7 0.0 copy-start.1
  0.7 0.7 copy-done.1
  1.4 0.0 copy-start.2
  1.4 94.5 %conv.1 = (bf16[128,512]{1,0:T(8,128)(2,1)S(1)}, f32[1,128]{1,0:T(1,128)S(1)}) custom-call(f32[3,3,512]{2,1,0:T(4,128)S(1)} %copy-done, f32[1,512]{1,0:T(1,128)S(1)} %bitcast.7, bf16[3,128,512]{2,1,0:T(8,128)(2,1)} %bitcast.9, f32[2,128,512]{2,1,0:T(8,128)} %filt_h.1, f32[2,6,512,128]{3,2,1,0:T(8,128)} %constant.4.clone.tabs_h, ...), custom_call_target="tpu_custom_call" | custom-call | tf_op jit(solution)/shard_map/conv/pallas_call | solution.py:367
  96.0 0.0 copy-done.2
  96.0 1.7 %fusion.1 = bf16[1,128,4096]{2,1,0:T(8,128)(2,1)} fusion(bf16[128,512]{1,0:T(8,128)(2,1)S(1)} %get-tuple-element.7, bf16[512,4096]{1,0:T(8,128)(2,1)S(1)} %copy-done.2, f32[128]{0:T(128)S(1)} %bitcast.8), kind=kOutput, calls=%fused_computation.2 | convolution fusion | flops 537919488 | bytes 5374464 | tf_op jit(solution)/shard_map/dot_general | solution.py:381
Async XLA Ops:
  0.0 0.7 copy-start
  0.7 0.7 copy-start.1
  1.4 94.6 %copy-start.2 = (bf16[512,4096]{1,0:T(8,128)(2,1)S(1)}, bf16[512,4096]{1,0:T(8,128)(2,1)}, u32[]{:S(2)}) copy-start(bf16[512,4096]{1,0:T(8,128)(2,1)} %param.11) | copy-start | bytes 12582916

commit v5 on v4

--- a/solution.py
+++ b/solution.py
@@ -14,17 +14,23 @@
 MESH = pl.DeviceIdType.MESH
 
 
-def tables(freqs, length):
-    q = np.arange(freqs, dtype=np.int64)[:, None]
+def tables(freqs, length, tile):
+    direct = np.arange(freqs // 2, dtype=np.int64).reshape(2, -1)
+    q = np.concatenate([direct, freqs - 1 - direct], axis=1).reshape(-1, 1)
     lane = np.arange(128, dtype=np.int64)[None]
 
     def circle(numerator, period):
         angles = 2.0 * np.pi * (numerator % period) / period
         return [np.cos(angles), -np.sin(angles)]
 
+    per, half = freqs // 4, tile // 2
+    block = min(128, per)
+    count = per // block
+    steps = 2 * tile * (lane // half) + 2 * (lane % half)
+    starts = 2 * tile * (lane % count) * (block // half) + tile * (lane // count % 2) + lane // (2 * count)
     twist = circle((2 * q + 1) * lane, 2 * length)
-    fine = circle((2 * q + 1) * lane, 4 * freqs)
-    coarse = circle((2 * q + 1) * lane * 128, 4 * freqs)
+    fine = circle((2 * q + 1) * steps, 4 * freqs)
+    coarse = circle((2 * q + 1) * starts, 4 * freqs)
     tabs = np.stack(twist + fine + coarse).reshape(6, 2, freqs // 2, 128).transpose(1, 0, 2, 3)
     cos, sin = circle(lane.T * lane, 128)
     forward = np.block([[cos, sin], [-sin, cos]])
@@ -51,15 +57,16 @@
 
 def kernel(Z, C, taps_h, skip_h, streams_h, filt_h, tabs_h, dft_h, out, scale,
            taps_w, skip, st, ft, tb, df, he, hr, sm0, sg, fx, fr, gx, gr, tmpf, tmps, zf, zs, xf, xs,
-           m1h, m1l, m2, hs, dc, yo, yr, zo, ro, tmpo, xo, rx,
+           m1h, m1l, m2, ps, hs, dc, yo, yr, zo, ro, tmpo, xo, rx,
            load, halo_s, halo_r, send, recv, reach):
     J = 128
     CH = Z * C
     S = 2 * CH
     QH = S // 2
-    QB = min(256, QH)
-    GB = min(128, QH)
-    SB = min(128, S)
+    QD, C2 = QH // 2, C // 2
+    PP = Z * C2
+    GB = min(128, QD)
+    SB = min(128, PP)
     ZP, CP = Z + 8, C + 8
     row, col = lax.axis_index("row"), lax.axis_index("col")
     z, core = row // 2, row % 2
@@ -144,6 +151,9 @@
                 device_id=(row, t), device_id_type=MESH).start()
             return carry
         lax.fori_loop(0, C - 1, body, 0, unroll=True)
+
+    def seat(c):
+        return c % 2 * C2 + c // 2
 
     def await_all(ref, sem):
         pltpu.make_async_copy(ref, ref, sem).wait()
@@ -199,46 +209,41 @@
     await_all(fr.at[pl.ds(0, C - 1)], recv.at[0])
     for h in range(2):
         for c in range(C):
-            tmpf[h, c * ZP:c * ZP + Z] = fr[c, h].astype(F32)
+            tmpf[h, seat(c) * ZP:seat(c) * ZP + Z] = fr[c, h].astype(F32)
     for h in range(2):
         for t in range(Z):
             zf[t, h] = tmpf[h, pl.ds(t, C, stride=ZP), :].astype(BF16)
-    to_z(zf, xf.at[z, core], 2, near_first)
-    xf[z, core] = zf[z]
+    to_z(zf, xf.at[core, z], 2, near_first)
+    xf[core, z] = zf[z]
     await_all(gr.at[pl.ds(0, C - 1)], recv.at[1])
     for c in range(C):
-        tmps[c * ZP:c * ZP + Z] = gr[c].astype(F32)
+        tmps[seat(c) * ZP:seat(c) * ZP + Z] = gr[c].astype(F32)
     for t in range(Z):
         zs[t] = tmps[pl.ds(t, C, stride=ZP), :].astype(BF16)
     hear(3)
-    to_z(zf, xf.at[z, core], 2, far_first)
+    to_z(zf, xf.at[core, z], 2, far_first)
     for k in range(4):
-        to_z(zs, xs.at[z, core], 3, lambda n, t, k=k: t % 4 == k)
-    xs[z, core] = zs[z]
+        to_z(zs, xs.at[core, z], 3, lambda n, t, k=k: t % 4 == k)
+    xs[core, z] = zs[z]
 
     loads[2].wait()
     loads[3].wait()
 
     def build(g, carry):
-        rows = pl.ds(pl.multiple_of(g * GB, GB), GB)
+        at_q = pl.multiple_of(g * GB, GB)
+        rows = pl.ds(at_q, GB)
         fine_re, fine_im = tb[2, rows, 0:SB], tb[3, rows, 0:SB]
         for a in range(S // SB):
             coarse_re, coarse_im = tb[4, rows, a:a + 1], tb[5, rows, a:a + 1]
             parts = (coarse_re * fine_re - coarse_im * fine_im, coarse_re * fine_im + coarse_im * fine_re)
             for k, part in enumerate(parts):
                 high, low = split(part)
-                per = QB // GB
-                where = pl.ds(pl.multiple_of((g % per) * GB, GB) + k * QB, GB)
-                m1h[g // per, where, a * SB:(a + 1) * SB] = high
-                m1l[g // per, where, a * SB:(a + 1) * SB] = low
-                flipped = part.T.astype(BF16)
-                for n in range(SB // C):
-                    tile = a * (SB // C) + n
-                    m2[tile % 2, (tile // 2) * C:(tile // 2 + 1) * C, pl.ds(pl.multiple_of(g * GB, GB) + k * QH, GB)] = (
-                        flipped[n * C:(n + 1) * C])
+                m1h[pl.ds(at_q + k * QD, GB), a * SB:(a + 1) * SB] = high
+                m1l[pl.ds(at_q + k * QD, GB), a * SB:(a + 1) * SB] = low
+                m2[a * SB:(a + 1) * SB, pl.ds(at_q + k * QD, GB)] = part.T.astype(BF16)
         return carry
 
-    lax.fori_loop(0, QH // GB, build, 0)
+    lax.fori_loop(0, QD // GB, build, 0)
 
     def to_mate(src, dst, k):
         pltpu.make_async_remote_copy(
@@ -249,56 +254,67 @@
         tw_re, tw_im = tb[0, rows], sign * tb[1, rows]
         return re * tw_re - im * tw_im, re * tw_im + im * tw_re
 
-    await_all(xf.at[pl.ds(0, Z - 1), 0], recv.at[2])
-    to_mate(xf.at[:, core], xf.at[:, core], 4)
-    await_all(xf.at[:, 0], recv.at[4])
-
-    def filter_rows(b, carry):
-        rows = pl.ds(pl.multiple_of(b * QB, QB), QB)
-        taps = jnp.concatenate([xf[:, :, h].reshape(S, J) for h in range(2)], axis=1)
-        p = dot(m1h[b], taps) + dot(m1l[b], taps)
-        sign = 1.0 - 2.0 * (lax.broadcasted_iota(jnp.int32, (QB, J), 0) % 2).astype(F32)
-        re = p[:QB, :J] - sign * p[QB:, J:]
-        im = p[QB:, :J] + sign * p[:QB, J:]
+    def both_halves(even, odd):
+        ere, eim, ore, oim = even[:QD], even[QD:], odd[:QD], odd[QD:]
+        return (ere + ore, eim + oim), (ere - ore, oim - eim)
+
+    halves = (slice(0, QD), slice(QD, QH))
+
+    await_all(xf.at[0, pl.ds(0, Z - 1)], recv.at[2])
+    to_mate(xf.at[core], xf.at[core], 4)
+    await_all(xf.at[0], recv.at[4])
+    sums = []
+    for k in range(2):
+        taps = jnp.concatenate([xf[:, :, h, k * C2:(k + 1) * C2].reshape(2 * PP, J) for h in range(2)], axis=1)
+        cols = slice(k * 2 * PP, (k + 1) * 2 * PP)
+        sums.append(dot(m1h[:, cols], taps) + dot(m1l[:, cols], taps))
+    sign = 1.0 - 2.0 * (lax.broadcasted_iota(jnp.int32, (QD, J), 0) % 2).astype(F32)
+    for rows, (re, im), flip in zip(halves, both_halves(*sums), (sign, -sign)):
+        re, im = re[:, :J] - flip * im[:, J:], im[:, :J] + flip * re[:, J:]
         hs[rows] = dot3(jnp.concatenate(twisted(re, im, rows, 1.0), axis=1), df[0])
-        return carry
-
-    lax.fori_loop(0, QH // QB, filter_rows, 0)
-
-    await_all(xs.at[pl.ds(0, Z - 1), 0], recv.at[3])
-    to_mate(xs.at[:, core], xs.at[:, core], 5)
-    await_all(xs.at[:, 0], recv.at[5])
-
-    def signal_rows(b, carry):
-        rows = pl.ds(pl.multiple_of(b * QB, QB), QB)
-        p = dot(m1h[b], xs[...].reshape(S, J))
-        g = dot3(jnp.concatenate(twisted(p[:QB], p[QB:], rows, 1.0), axis=1), df[0])
+
+    await_all(xs.at[0, pl.ds(0, Z - 1)], recv.at[3])
+    to_mate(xs.at[core], xs.at[core], 5)
+
+    def partial(k, who):
+        cols = pl.ds(pl.multiple_of(k * 2 * PP + who * PP, PP), PP)
+        return dot(m1h[:, cols], xs[who, :, k * C2:(k + 1) * C2].reshape(PP, J))
+
+    for k in range(2):
+        ps[k] = partial(k, core)
+    await_all(xs.at[0], recv.at[5])
+    sums = [ps[k] + partial(k, 1 - core) for k in range(2)]
+    back = []
+    for rows, (re, im) in zip(halves, both_halves(*sums)):
+        g = dot3(jnp.concatenate(twisted(re, im, rows, 1.0), axis=1), df[0])
         h = hs[rows]
         gre, gim, hre, him = g[:, :J], g[:, J:], h[:, :J], h[:, J:]
         y = dot3(jnp.concatenate([gre * hre - gim * him, gre * him + gim * hre], axis=1), df[1])
-        parts = twisted(y[:, :J], y[:, J:], rows, -1.0)
-        for k, part in enumerate(parts):
-            high, low = split(part * (1.0 / (S * J)))
-            where = pl.ds(pl.multiple_of(b * QB, QB) + k * QH, QB)
-            dc[where, 0:J] = high
-            dc[where, J:2 * J] = low
-        return carry
-
-    lax.fori_loop(0, QH // QB, signal_rows, 0, unroll=True)
-    other = dot(m2[1 - core], dc[...])
-    yo[...] = (other[:, :J] + other[:, J:]).reshape(Z, C, J)
+        back.append([part * (1.0 / (S * J)) for part in twisted(y[:, :J], y[:, J:], rows, -1.0)])
+    (dre, dim), (mre, mim) = back
+    for k, parts in enumerate(((dre + mre, dim - mim), (dre - mre, dim + mim))):
+        for n, part in enumerate(parts):
+            high, low = split(part)
+            dc[k, n * QD:(n + 1) * QD, 0:J] = high
+            dc[k, n * QD:(n + 1) * QD, J:2 * J] = low
+
+    def positions(k, who):
+        y = dot(m2[pl.ds(pl.multiple_of(k * 2 * PP + who * PP, PP), PP), :], dc[k])
+        return (y[:, :J] + y[:, J:]).reshape(Z, C2, J)
+
+    for k in range(2):
+        yo[:, k * C2:(k + 1) * C2] = positions(k, 1 - core)
     to_mate(yo, yr, 6)
-    own = dot(m2[core], dc[...])
-    own = (own[:, :J] + own[:, J:]).reshape(Z, C, J)
+    own = [positions(k, core) for k in range(2)]
     await_all(yr, recv.at[6])
-    zo[...] = (own + yr[...]).astype(BF16)
+    zo[...] = (jnp.concatenate(own, axis=1) + yr[...]).astype(BF16)
     to_z(zo, ro.at[z], 7)
     ro[z] = zo[z]
     await_all(ro.at[pl.ds(0, Z - 1)], recv.at[7])
     for t in range(Z):
         tmpo[t * CP:t * CP + C] = ro[t].astype(F32)
     for c in range(C):
-        xo[c] = tmpo[pl.ds(c, Z, stride=CP), :].astype(BF16)
+        xo[c] = tmpo[pl.ds(seat(c), Z, stride=CP), :].astype(BF16)
     to_c(xo, rx.at[col], 8)
     rx[col] = xo[col]
     await_all(rx.at[pl.ds(0, C - 1)], recv.at[8])
@@ -311,7 +327,7 @@
     for c in halos:
         c.wait_send()
     for ref, k in ((fx.at[pl.ds(0, C - 1)], 0), (gx.at[pl.ds(0, C - 1)], 1), (zf.at[pl.ds(0, Z - 1)], 2),
-                   (zs.at[pl.ds(0, Z - 1)], 3), (xf.at[:, 0], 4), (xs.at[:, 0], 5), (yo, 6),
+                   (zs.at[pl.ds(0, Z - 1)], 3), (xf.at[0], 4), (xs.at[0], 5), (yo, 6),
                    (zo.at[pl.ds(0, Z - 1)], 7), (xo.at[pl.ds(0, C - 1)], 8)):
         await_all(ref, send.at[k])
 
@@ -320,8 +336,7 @@
     J, CH = 128, Z * C
     S = 2 * CH
     QH = S // 2
-    QB = min(256, QH)
-    tabs, dfts = tables(S, 2 * S * J)
+    tabs, dfts = tables(S, 2 * S * J, C)
     vmem = pltpu.VMEM
     scratch = [
         vmem((3, 3, CH), F32),
@@ -342,13 +357,14 @@
         vmem((C * (Z + 8), J), F32),
         vmem((Z, 2, C, J), BF16),
         vmem((Z, C, J), BF16),
-        vmem((Z, 2, 2, C, J), BF16),
-        vmem((Z, 2, C, J), BF16),
-        vmem((QH // QB, 2 * QB, S), BF16),
-        vmem((QH // QB, 2 * QB, S), BF16),
-        vmem((2, S // 2, 2 * QH), BF16),
+        vmem((2, Z, 2, C, J), BF16),
+        vmem((2, Z, C, J), BF16),
+        vmem((QH, S), BF16),
+        vmem((QH, S), BF16),
+        vmem((S, QH), BF16),
+        vmem((2, QH, J), F32),
         vmem((QH, 2 * J), F32),
-        vmem((2 * QH, 2 * J), BF16),
+        vmem((2, QH, 2 * J), BF16),
         vmem((Z, C, J), F32),
         vmem((Z, C, J), F32),
         vmem((Z, C, J), BF16),

time: 97.9 us -> 96.6 us (0.987)
  Pallas kernels: 94.5 us -> 93.2 us
    pallas_call x1, Pallas kernels: 94.5 us -> 93.2 us  [convolve(): pl.pallas_call(functools.partial(kernel, Z, C), out_shape=[jax.ShapeDtype...]
where the time goes in v5:
time: 96.6 us; the launch traced here: 96.4 us
  Pallas kernels  93.2 us (96%)
  matrix products  1.74 us (2%)
  local copies, waits for them, and re-layouts  1.42 us (1%)
    pallas_call x1, Pallas kernels, convolve(): pl.pallas_call(functools.partial(kernel, Z, C), out_shape=[jax.ShapeDtype...  93.2 us

profile of v5, /device:TPU:1, one launch (start us, length us, event | category | flops | bytes accessed | tf_op | source)
XLA Modules:
  0.0 96.4 jit_solution(2070556543761911017)
XLA Ops:
  0.0 0.0 copy-start
  0.0 0.7 copy-done
  0.7 0.0 copy-start.1
  0.7 0.7 copy-done.1
  1.4 0.0 copy-start.2
  1.4 93.2 %conv.1 = (bf16[128,512]{1,0:T(8,128)(2,1)S(1)}, f32[1,128]{1,0:T(1,128)S(1)}) custom-call(f32[3,3,512]{2,1,0:T(4,128)S(1)} %copy-done, f32[1,512]{1,0:T(1,128)S(1)} %bitcast.7, bf16[3,128,512]{2,1,0:T(8,128)(2,1)} %bitcast.9, f32[2,128,512]{2,1,0:T(8,128)} %filt_h.1, f32[2,6,512,128]{3,2,1,0:T(8,128)} %constant.4.clone.tabs_h, ...), custom_call_target="tpu_custom_call" | custom-call | tf_op jit(solution)/shard_map/conv/pallas_call | solution.py:383
  94.7 0.0 copy-done.2
  94.7 1.7 %fusion.1 = bf16[1,128,4096]{2,1,0:T(8,128)(2,1)} fusion(bf16[128,512]{1,0:T(8,128)(2,1)S(1)} %get-tuple-element.7, bf16[512,4096]{1,0:T(8,128)(2,1)S(1)} %copy-done.2, f32[128]{0:T(128)S(1)} %bitcast.8), kind=kOutput, calls=%fused_computation.2 | convolution fusion | flops 537919488 | bytes 5374464 | tf_op jit(solution)/shard_map/dot_general | solution.py:397
Async XLA Ops:
  0.0 0.7 copy-start
  0.7 0.7 copy-start.1
  1.4 93.3 %copy-start.2 = (bf16[512,4096]{1,0:T(8,128)(2,1)S(1)}, bf16[512,4096]{1,0:T(8,128)(2,1)}, u32[]{:S(2)}) copy-start(bf16[512,4096]{1,0:T(8,128)(2,1)} %param.11) | copy-start | bytes 12582916
